TPU v7x, 256 devices: a whole 4x4x8 slice. The times are simulated.
256 devices in a mesh: sp: 64 (over z, y, core), tp: 4 (over x).
Axes of the slice: x: 4, y: 4, z: 8, core: 2. Of those that a mesh axis runs over, the one named last changes fastest.
Arguments:
- tokens: bfloat16 [49152, 2048], P('sp', 'tp'), may hold values from -12 to 12
- query_weight: bfloat16 [2048, 1024], P('sp', 'tp'), may hold values from -0.176776695 to 0.176776695
- key_projection: bfloat16 [2048, 512], P('sp', 'tp'), may hold values from -0.176776695 to 0.176776695
- value_projection: bfloat16 [2048, 512], P('sp', 'tp'), may hold values from -0.125 to 0.125
- conv_in_weight: bfloat16 [2048, 1024], P('sp', 'tp'), may hold values from -0.125 to 0.125
- conv_gate_out: bfloat16 [2048, 1024], P('sp', 'tp'), may hold values from -0.125 to 0.125
- conv_gate_in: bfloat16 [2048, 1024], P('sp', 'tp'), may hold values from -0.125 to 0.125
- conv_taps: bfloat16 [3, 1024], P(None, 'tp'), may hold values from -3 to 3
- head_sink_logit: float32 [8], P('tp'), may hold values from 3 to 8
- out_attn_weight: bfloat16 [1024, 2048], P('tp', 'sp'), may hold values from -5 to 5
- out_conv_weight: bfloat16 [1024, 2048], P('tp', 'sp'), may hold values from -0.5 to 0.5
- out_gain: float32 [2048], P('tp'), may hold values from 0.1 to 1.9
Outputs:
- mixed: bfloat16 [49152, 2048], P('sp', 'tp')
All inputs are finite; a program needn't handle non-finite values.
Results may differ from a plain program's by a relative error of at most 0.014.
Values may be sent and summed in bfloat16 or wider, within the bound.
A program may use at most 64 MiB of HBM per device.

v0:
```python
import jax
import jax.numpy as jnp
from jax import lax
from jax.sharding import PartitionSpec as P

HEAD_SIZE = 128
WINDOW = 128
GRID = 64


NEG_BIG = -1e30
THETA = 10000.0
EPS = 1e-05


def with_halo(block, sides, width):
    for axis, dim in sides:
        count = lax.axis_size(axis)
        forward = [(i, i + 1) for i in range(count - 1)]
        backward = [(target, source) for source, target in forward]
        low = lax.ppermute(
            lax.slice_in_dim(block, block.shape[dim] - width, None, axis=dim), axis, forward
        )
        high = lax.ppermute(lax.slice_in_dim(block, 0, width, axis=dim), axis, backward)
        block = jnp.concatenate([low, block, high], axis=dim)
    return block


def in_order(blocks, dim):
    lengths = list(blocks.shape[1:])
    lengths[dim] *= blocks.shape[0]
    return jnp.moveaxis(blocks, 0, dim).reshape(lengths)


def copy_for_each(array, axis):
    copies = jnp.broadcast_to(array, (lax.axis_size(axis), *array.shape))
    return lax.all_to_all(copies, axis, split_axis=0, concat_axis=0, tiled=True)


def gather_directly(array, axis, dim):
    return in_order(copy_for_each(array, axis), dim)


def sent_together(arrays, axis, dim, along):
    ends, at = ([], 0)
    for a in arrays[:-1]:
        at += a.shape[along]
        ends.append(at)
    both = jnp.concatenate(arrays, axis=along)
    return tuple(jnp.split(lax.all_gather(both, axis, axis=dim, tiled=True), ends, axis=along))


def cut_along(array, dim, size):
    lengths = array.shape
    blocks = array.reshape(*lengths[:dim], size, lengths[dim] // size, *lengths[dim + 1 :])
    return jnp.moveaxis(blocks, dim, 0)


def sum_at_owner(array, axis, dim):
    blocks = cut_along(array, dim, lax.axis_size(axis))
    arrived = lax.all_to_all(blocks, axis, split_axis=0, concat_axis=0, tiled=True)
    return arrived.astype(jnp.float32).sum(axis=0)


def over_copies(array, axis):
    return copy_for_each(array, axis).sum(axis=0)


def in_one(arrays, axis):
    flat, at, finished = (jnp.concatenate([a.reshape(-1) for a in arrays]), 0, [])
    so_far = over_copies(flat, axis)
    for a in arrays:
        finished.append(so_far[at : at + a.size].reshape(a.shape))
        at += a.size
    return tuple(finished)


def rope_tables(positions):
    row = (positions // GRID).astype(jnp.float32)
    column = (positions % GRID).astype(jnp.float32)
    half = HEAD_SIZE // 2
    inverse = THETA ** (-jnp.arange(0, half, 2, dtype=jnp.float32) / half)
    angle_row = row[:, None] * inverse
    angle_col = column[:, None] * inverse
    angles = jnp.concatenate([angle_row, angle_row, angle_col, angle_col], -1)
    return (jnp.cos(angles)[:, None, :], jnp.sin(angles)[:, None, :])


def rotate(vectors, cosine, sine):
    first, second, third, fourth = jnp.split(vectors, 4, axis=-1)
    turned = jnp.concatenate([-second, first, -fourth, third], -1)
    return vectors * cosine + turned * sine


def attend(query_vectors, paired, head_sink_logit, offset, total_tokens):
    item_count = query_vectors.shape[0]
    kv_heads = paired.shape[1] // (2 * HEAD_SIZE)
    head_group = query_vectors.shape[1] // (kv_heads * HEAD_SIZE)
    blocks = item_count // WINDOW
    padded = with_halo(paired, (("sp", 0),), WINDOW)
    shaped = padded.reshape(blocks + 2, WINDOW, paired.shape[1])
    banded = jnp.concatenate([shaped[:-2], shaped[1:-1], shaped[2:]], axis=1)
    banded = banded.reshape(blocks, 3 * WINDOW, 2, kv_heads, HEAD_SIZE)
    key_band = banded[:, :, 0]
    value_band = banded[:, :, 1]
    query_blocks = query_vectors.reshape(blocks, WINDOW, kv_heads, head_group, HEAD_SIZE)
    scores = jnp.einsum(
        "nqhgd,nkhd->nhgqk", query_blocks, key_band, preferred_element_type=jnp.float32
    ) * HEAD_SIZE ** (-0.5)
    block_start = offset + jnp.arange(blocks, dtype=jnp.int32)[:, None] * WINDOW
    query_pos = block_start + jnp.arange(WINDOW, dtype=jnp.int32)[None, :]
    key_pos = block_start - WINDOW + jnp.arange(3 * WINDOW, dtype=jnp.int32)[None, :]
    distance = key_pos[:, None, :] - query_pos[:, :, None]
    valid = (
        (jnp.abs(distance) <= WINDOW)
        & (key_pos[:, None, :] >= 0)
        & (key_pos[:, None, :] < total_tokens)
    )
    scores = jnp.where(valid[:, None, None], scores, NEG_BIG)
    sink_col = head_sink_logit.reshape(1, kv_heads, head_group, 1, 1)
    top = jnp.maximum(jnp.max(scores, -1, keepdims=True), sink_col)
    weights = jnp.exp(scores - top)
    denominator = jnp.sum(weights, -1, keepdims=True) + jnp.exp(sink_col - top)
    probs = (weights / denominator).astype(jnp.bfloat16)
    mixed_heads = jnp.einsum(
        "nhgqk,nkhd->nqhgd", probs, value_band, preferred_element_type=jnp.float32
    )
    return mixed_heads.reshape(item_count, kv_heads * head_group * HEAD_SIZE).astype(jnp.bfloat16)


def convolve(gate_before, conv_input, gate_after, conv_taps):
    sectioned = (gate_before * conv_input).astype(jnp.bfloat16)
    bordered = with_halo(sectioned, (("sp", 0),), 1)
    taps = conv_taps.astype(jnp.float32)
    conv_mix = bordered[:-2] * taps[0] + bordered[1:-1] * taps[1] + bordered[2:] * taps[2]
    return (gate_after * conv_mix).astype(jnp.bfloat16)


def body(
    tokens,
    query_weight,
    key_projection,
    value_projection,
    conv_in_weight,
    conv_gate_out,
    conv_gate_in,
    conv_taps,
    head_sink_logit,
    out_attn_weight,
    out_conv_weight,
    out_gain,
):
    whole = gather_directly(tokens, "tp", 1)
    item_count = whole.shape[0]
    offset = lax.axis_index("sp") * item_count
    total_tokens = item_count * lax.axis_size("sp")
    positions = offset + jnp.arange(item_count, dtype=jnp.int32)
    cosine, sine = rope_tables(positions)
    pieces = sent_together(
        (
            query_weight,
            key_projection,
            value_projection,
            conv_in_weight,
            conv_gate_out,
            conv_gate_in,
        ),
        "sp",
        0,
        1,
    )
    query_raw, key_unrotated, value_raw, conv_input, gate_after, gate_before = tuple(
        (jnp.dot(whole, piece, preferred_element_type=jnp.float32) for piece in pieces)
    )
    query_vectors = (
        rotate(query_raw.reshape(item_count, -1, HEAD_SIZE), cosine, sine)
        .reshape(item_count, -1)
        .astype(jnp.bfloat16)
    )
    key_rows = (
        rotate(key_unrotated.reshape(item_count, -1, HEAD_SIZE), cosine, sine)
        .reshape(item_count, -1)
        .astype(jnp.bfloat16)
    )
    paired = jnp.concatenate([key_rows, value_raw.astype(jnp.bfloat16)], 1)
    attention_out = attend(query_vectors, paired, head_sink_logit, offset, total_tokens)
    conv_out = convolve(gate_before, conv_input, gate_after, conv_taps)
    mixer_rows = jnp.concatenate([attention_out, conv_out], 1)
    stacked = jnp.concatenate([out_attn_weight, out_conv_weight], 0)
    own_width = out_gain.shape[0]
    partial_sums = jnp.dot(
        mixer_rows, gather_directly(stacked, "sp", 1), preferred_element_type=jnp.float32
    )
    summed = sum_at_owner(partial_sums.astype(jnp.bfloat16), "tp", 1)
    full_width = own_width * lax.axis_size("tp")
    first_sum, square_sum = in_one((jnp.sum(summed, 1), jnp.sum(summed * summed, 1)), "tp")
    mean = first_sum / full_width
    spread = square_sum / full_width - mean * mean
    normed = (summed - mean[:, None]) * lax.rsqrt(spread[:, None] + EPS) * out_gain
    return normed.astype(jnp.bfloat16)


def solution(mesh):
    return jax.shard_map(
        body,
        mesh=mesh,
        in_specs=(
            P("sp", "tp"),
            P("sp", "tp"),
            P("sp", "tp"),
            P("sp", "tp"),
            P("sp", "tp"),
            P("sp", "tp"),
            P("sp", "tp"),
            P(None, "tp"),
            P("tp"),
            P("tp", "sp"),
            P("tp", "sp"),
            P("tp"),
        ),
        out_specs=P("sp", "tp"),
        check_vma=False,
    )
```

profile of v0, /device:TPU:2, one launch (start us, length us, event | category | flops | bytes accessed | tf_op | source)
XLA Modules:
  0.0 204.1 jit_solution(6715690389183473567)
XLA Ops:
  11.5 1.4 copy.61
  12.9 1.9 broadcast_in_dim.14
  14.8 6.0 %all-to-all-start = ((bf16[4,768,512]{1,2,0:T(8,128)(2,1)}), bf16[4,768,512]{1,2,0:T(8,128)(2,1)S(1)}, u32[]{:S(2)}, u32[]{:S(2)}) async-start(bf16[4,768,512]{1,2,0:T(8,128)(2,1)} %broadcast_in_dim.14), calls=%async_computation | async-start | bytes 6291456 | tf_op jit(solution)/shard_map/all_to_all | solution.py:37
  21.2 2.8 %fusion.7 = pred[6,128,384]{1,2,0:T(8,128)(4,1)} fusion(s32[6,128]{1,0:T(8,128)S(1)} %iota_add_fusion.1, s32[6,384]{1,0:T(8,128)S(1)} %iota_add_fusion, pred[6,384]{1,0:T(8,128)(4,1)S(1)} %get-tuple-element.31, pred[6,384]{1,0:T(8,128)(4,1)S(1)} %get-tuple-element.30), kind=kLoop, calls=%fused_computation.21 | loop fusion | flops 1474560 | bytes 311808 | tf_op jit(solution)/shard_map/and | solution.py:115
  24.0 31.9 %all-to-all-done = bf16[4,768,512]{1,2,0:T(8,128)(2,1)S(1)} async-done(((bf16[4,768,512]{1,2,0:T(8,128)(2,1)}), bf16[4,768,512]{1,2,0:T(8,128)(2,1)S(1)}, u32[]{:S(2)}, u32[]{:S(2)}) %all-to-all-start) | async-done | bytes 3145760 | tf_op jit(solution)/shard_map/all_to_all | solution.py:37
  55.8 1.6 broadcast_in_dim.17
  57.5 12.4 %all-to-all-start.1 = ((bf16[64,512,32]{1,2,0:T(8,128)(2,1)}), bf16[64,512,32]{1,2,0:T(8,128)(2,1)}, u32[]{:S(2)}, u32[]{:S(2)}) async-start(bf16[64,512,32]{1,2,0:T(8,128)(2,1)} %broadcast_in_dim.17), calls=%async_computation.1 | async-start | bytes 4194304 | tf_op jit(solution)/shard_map/all_to_all | solution.py:37
  69.9 40.7 %all-gather.2.cloned.1.call-done = bf16[2048,1280]{1,0:T(8,128)(2,1)} async-done(((bf16[32,1280]{1,0:T(8,128)(2,1)}), bf16[2048,1280]{1,0:T(8,128)(2,1)}) %all-gather.2.cloned.1.call-update) | async-done | bytes 5242896 | tf_op jit(solution)/shard_map/all_gather | solution.py:50
  110.6 1.8 fusion.22
  112.4 1.5 fusion.28
  115.2 2.8 %collective-permute-start = (bf16[128,256]{0,1:T(8,128)(2,1)}, bf16[128,256]{0,1:T(8,128)(2,1)}, u32[]{:S(2)}, u32[]{:S(2)}) collective-permute-start(bf16[128,256]{0,1:T(8,128)(2,1)} %get-tuple-element.14), channel_id=1, source_target_pairs={{0,4},{4,8},{8,12},{12,16},{16,20},{20,24},{24,28},{28,32},{32,36}... | collective-permute-start | bytes 196616 | tf_op jit(solution)/shard_map/ppermute | solution.py:21
  118.0 1.3 collective-permute-start.1
  119.3 1.0 fusion.11
  120.3 1.0 fusion.3
  122.1 3.6 %collective-permute-start.2 = (bf16[1,256]{0,1:T(8,128)(2,1)}, bf16[1,256]{0,1:T(8,128)(2,1)}, u32[]{:S(2)}, u32[]{:S(2)}) collective-permute-start(bf16[1,256]{0,1:T(8,128)(2,1)} %get-tuple-element.20), channel_id=1, source_target_pairs={{0,4},{4,8},{8,12},{12,16},{16,20},{20,24},{24,28},{28,32},{32,36}... | collective-permute-start | bytes 1544 | tf_op jit(solution)/shard_map/ppermute | solution.py:21
  125.8 1.5 collective-permute-start.3
  127.3 1.0 fusion.14
  129.3 2.2 %reshape.342 = bf16[6,128,2,128]{1,0,3,2:T(8,128)(2,1)} reshape(bf16[768,256]{0,1:T(8,128)(2,1)} %fusion.19) | data formatting | bytes 786432 | tf_op jit(solution)/shard_map/reshape.5
  131.5 3.4 %multiply_convert_fusion.1 = bf16[768,256]{0,1:T(8,128)(2,1)} fusion(bf16[768,256]{0,1:T(8,128)(2,1)} %copy-done.4, bf16[1,256]{0,1:T(8,128)(2,1)} %collective-permute-done.3, bf16[1,256]{0,1:T(8,128)(2,1)} %collective-permute-done.2, f32[256]{0:T(256)S(1)} %bitcast.120, f32[256]{0:T(256)S(1)} %bitcast.119, f32[256]{0:T(256)S(1)} %bitcast.118, ...), kind=kOutput, calls=%fused_computation.38 | convolution fusion | flops 808452096 | bytes 5114880 | tf_op jit(solution)/shard_map/dot_general | solution.py:173
  134.9 1.0 pad_maximum_fusion.6
  141.0 3.4 %convolution_convert_fusion = bf16[768,2048]{1,0:T(8,128)(2,1)S(1)} fusion(bf16[512,2048]{0,1:T(8,128)(2,1)} %bitcast.32, bf16[768,256]{0,1:T(8,128)(2,1)S(1)} %copy-done.10, bf16[768,256]{0,1:T(8,128)(2,1)S(1)} %bitcast.117), kind=kOutput, calls=%fused_computation.2 | convolution fusion | flops 1613758464 | bytes 6029312 | tf_op jit(solution)/shard_map/dot_general | solution.py:191
  144.8 42.6 %all_to_all.21 = bf16[4,768,512]{2,1,0:T(8,128)(2,1)S(1)} all-to-all(bf16[4,768,512]{2,1,0:T(8,128)(2,1)S(1)} %bitcast.112), channel_id=1, replica_groups=mesh['sp'=64,'tp'=4] {'tp'}, dimensions={0} | all-to-all | bytes 6291456 | tf_op jit(solution)/shard_map/all_to_all | solution.py:61
  188.3 7.8 %all_to_all.22 = f32[4,1,1536]{2,1,0:T(1,128)S(1)} all-to-all(f32[4,1,1536]{2,1,0:T(1,128)S(1)} %broadcast_in_dim.18), channel_id=1, replica_groups=mesh['sp'=64,'tp'=4] {'tp'}, dimensions={0} | all-to-all | bytes 49152 | tf_op jit(solution)/shard_map/all_to_all | solution.py:37
  196.1 1.2 multiply_convert_fusion
  (72 shorter events, 14.6 us)
Async XLA Ops:
  6.5 104.0 %all-gather.2.cloned.1.call-start = ((), (), s32[]{:S(2)}) async-start(), calls=%async_computation.4 | async-start | bytes 5324800 | tf_op jit(solution)/shard_map/all_gather | solution.py:50
  10.8 0.6 copy-start.3
  14.8 6.1 %copy-start.5 = (bf16[256,32]{0,1:T(8,128)(2,1)S(1)}, bf16[256,32]{0,1:T(8,128)(2,1)}, u32[]{:S(2)}) copy-start(bf16[256,32]{0,1:T(8,128)(2,1)} %param.22) | copy-start | bytes 49156
  14.8 6.1 %copy-start.6 = (bf16[256,32]{0,1:T(8,128)(2,1)S(1)}, bf16[256,32]{0,1:T(8,128)(2,1)}, u32[]{:S(2)}) copy-start(bf16[256,32]{0,1:T(8,128)(2,1)} %param.21) | copy-start | bytes 49156
  14.8 6.2 %copy-start.7 = (bf16[3,256]{1,0:T(4,128)(2,1)S(1)}, bf16[3,256]{1,0:T(4,128)(2,1)}, u32[]{:S(2)}) copy-start(bf16[3,256]{1,0:T(4,128)(2,1)} %param.19) | copy-start | bytes 4612
  14.8 41.1 %all-to-all-start = ((bf16[4,768,512]{1,2,0:T(8,128)(2,1)}), bf16[4,768,512]{1,2,0:T(8,128)(2,1)S(1)}, u32[]{:S(2)}, u32[]{:S(2)}) async-start(bf16[4,768,512]{1,2,0:T(8,128)(2,1)} %broadcast_in_dim.14), calls=%async_computation | async-start | bytes 6291456 | tf_op jit(solution)/shard_map/all_to_all | solution.py:37
  57.5 83.5 %all-to-all-start.1 = ((bf16[64,512,32]{1,2,0:T(8,128)(2,1)}), bf16[64,512,32]{1,2,0:T(8,128)(2,1)}, u32[]{:S(2)}, u32[]{:S(2)}) async-start(bf16[64,512,32]{1,2,0:T(8,128)(2,1)} %broadcast_in_dim.17), calls=%async_computation.1 | async-start | bytes 4194304 | tf_op jit(solution)/shard_map/all_to_all | solution.py:37
  110.6 3.4 %copy-start.2 = (bf16[2048,1280]{1,0:T(8,128)(2,1)S(1)}, bf16[2048,1280]{1,0:T(8,128)(2,1)}, u32[]{:S(2)}) copy-start(bf16[2048,1280]{1,0:T(8,128)(2,1)} %all-gather.2.cloned.1.call-done) | copy-start | bytes 15728644
  115.2 19.7 %collective-permute-start = (bf16[128,256]{0,1:T(8,128)(2,1)}, bf16[128,256]{0,1:T(8,128)(2,1)}, u32[]{:S(2)}, u32[]{:S(2)}) collective-permute-start(bf16[128,256]{0,1:T(8,128)(2,1)} %get-tuple-element.14), channel_id=1, source_target_pairs={{0,4},{4,8},{8,12},{12,16},{16,20},{20,24},{24,28},{28,32},{32,36}... | collective-permute-start | bytes 196616 | tf_op jit(solution)/shard_map/ppermute | solution.py:21
  118.0 16.9 %collective-permute-start.1 = (bf16[128,256]{0,1:T(8,128)(2,1)}, bf16[128,256]{0,1:T(8,128)(2,1)}, u32[]{:S(2)}, u32[]{:S(2)}) collective-permute-start(bf16[128,256]{0,1:T(8,128)(2,1)} %get-tuple-element.15), channel_id=1, source_target_pairs={{4,0},{8,4},{12,8},{16,12},{20,16},{24,20},{28,24},{32,28},{36,32}... | collective-permute-start | bytes 196616 | tf_op jit(solution)/shard_map/ppermute | solution.py:24
  121.3 7.0 %copy-start.4 = (bf16[768,256]{0,1:T(8,128)(2,1)}, bf16[768,256]{0,1:T(8,128)(2,1)S(1)}, u32[]{:S(2)}) copy-start(bf16[768,256]{0,1:T(8,128)(2,1)S(1)} %fusion.3) | copy-start | bytes 1179652
  122.1 9.4 %collective-permute-start.2 = (bf16[1,256]{0,1:T(8,128)(2,1)}, bf16[1,256]{0,1:T(8,128)(2,1)}, u32[]{:S(2)}, u32[]{:S(2)}) collective-permute-start(bf16[1,256]{0,1:T(8,128)(2,1)} %get-tuple-element.20), channel_id=1, source_target_pairs={{0,4},{4,8},{8,12},{12,16},{16,20},{20,24},{24,28},{28,32},{32,36}... | collective-permute-start | bytes 1544 | tf_op jit(solution)/shard_map/ppermute | solution.py:21
  125.8 5.7 %collective-permute-start.3 = (bf16[1,256]{0,1:T(8,128)(2,1)}, bf16[1,256]{0,1:T(8,128)(2,1)}, u32[]{:S(2)}, u32[]{:S(2)}) collective-permute-start(bf16[1,256]{0,1:T(8,128)(2,1)} %get-tuple-element.21), channel_id=1, source_target_pairs={{4,0},{8,4},{12,8},{16,12},{20,16},{24,20},{28,24},{32,28},{36,32}... | collective-permute-start | bytes 1544 | tf_op jit(solution)/shard_map/ppermute | solution.py:24
  137.2 1.3 copy-start
  137.2 1.3 copy-start.1
  138.4 0.7 copy-start.8
  139.8 1.2 copy-start.10
  187.4 8.7 %copy-start.9 = (f32[512]{0:T(512)S(1)}, f32[512]{0:T(512)}, u32[]{:S(2)}) copy-start(f32[512]{0:T(512)} %param.23) | copy-start | bytes 6148
Sparse Core Ops, SparseCore 0:
  11.6 98.9 all-gather.1
where the time goes:
time: 208 us; the launch traced here: 204 us
  waiting for transfers between devices  72.6 us (35%)
  blocking collectives  50.4 us (24%)
  starting transfers between devices  27.6 us (13%)
  local copies, waits for them, and re-layouts  16.1 us (8%)
  between operations  13.8 us (7%)
  matrix products  13.7 us (7%)
  other arithmetic  10.1 us (5%)
    all_to_all x1, blocking collectives, sum_at_owner(): lax.all_to_all(blocks, axis, split_axis=0, concat_axis=0, tiled=True)  42.6 us
    all_gather x1, waiting for transfers between devices, sent_together(): lax.all_gather(both, axis, axis=dim, tiled=True)  40.7 us
    all_to_all x2, waiting for transfers between devices, copy_for_each(): return lax.all_to_all(copies, axis, split_axis=0, concat_axis=0, tiled=True)  31.9 us
    all_to_all x2, starting transfers between devices, copy_for_each(): return lax.all_to_all(copies, axis, split_axis=0, concat_axis=0, tiled=True)  18.4 us
    dot_general x6, matrix products, body(): jnp.dot(whole, piece, preferred_element_type=jnp.float32)  8.89 us
    all_to_all x1, blocking collectives, copy_for_each(): return lax.all_to_all(copies, axis, split_axis=0, concat_axis=0, tiled=True)  7.76 us
    ppermute x2, starting transfers between devices, with_halo(): lax.ppermute(lax.slice_in_dim(block, block.shape[dim] - width, None, axis...  6.4 us
    unnamed x29, local copies, waits for them, and re-layouts  5.85 us
  transfers between devices with their start and end apart: 7, of which 2 were waited for; matrix products, arithmetic and copies ran while one was open for 14% of the time, Pallas kernels for 0%

commit v1 on v0

v1 whole, which is shorter than its diff:
```python
import functools

import jax
import jax.numpy as jnp
import numpy as np
from jax import lax
from jax.experimental import pallas as pl
from jax.experimental.pallas import tpu as pltpu
from jax.sharding import PartitionSpec as P

MESH = pl.DeviceIdType.MESH
F32 = jnp.float32
BF16 = jnp.bfloat16

HEAD = 128
WINDOW = 128
GRID = 64
NEG_BIG = -1e30
THETA = 10000.0
EPS = 1e-05

NZ, NY, NX, NSP = 8, 4, 4, 64
ROWS = 768
WIDTH = 2048
QUARTER = 512
CA = 768
CB = 1024
ORDER = (0, 5, 1, 2, 3, 4)
CHUNKS = ((0, 128, 0), (128, 128, 640), (256, 256, 128), (512, 256, 384))


def nt_dot(a, b):
    return lax.dot_general(a, b, (((1,), (1,)), ((), ())), preferred_element_type=F32)


def kernel(
    tok, qw, kw, vw, cin, cgo, cgi, taps_in, sink, owa, owc, gain_in, freq_in, out,
    T, WA, WB, KV, Q, SEC, GA, MIX, ES, ER, COS, SIN, S2, PT, PB, PX, S1, R2, R1, ST, OUT,
    owa_v, owc_v, taps_v, gain_v, freq_v,
    lsem, ssem, wrec, srec, irec, xrec, hrec, r2rec, r1rec, strec, osem,
):
    s = lax.axis_index("sp")
    x = lax.axis_index("tp")
    core = s % 2
    chip = s // 2
    y = chip % NY
    z = chip // NY

    def at(zz, yy, cc):
        return ((zz % NZ) * NY + yy % NY) * 2 + cc

    sib = (at(z, y, 1 - core), x)
    yp, ym, y2 = [(at(z, y + d, core), x) for d in (1, 3, 2)]
    zp, zm = [(at(z + d, y, core), x) for d in (1, NZ - 1)]
    xp, xm, x2 = [(s, (x + d) % NX) for d in (1, 3, 2)]
    sp, sm = [((s + d) % NSP, x) for d in (1, NSP - 1)]

    loads = []

    def load(src, dst):
        cp = pltpu.make_async_copy(src, dst, lsem.at[len(loads)])
        cp.start()
        loads.append(cp)
        return cp

    own_cols = pl.ds(pl.multiple_of(x * QUARTER, QUARTER), QUARTER)
    own_rows = pl.ds(pl.multiple_of(core * 32, 32), 32)
    l_out = [load(owa, owa_v), load(owc, owc_v)]
    l_w = [
        load(qw, WA.at[z, y, own_rows, pl.ds(0, 256)]),
        load(kw, WA.at[z, y, own_rows, pl.ds(256, 128)]),
        load(vw, WA.at[z, y, own_rows, pl.ds(384, 128)]),
        load(cin, WB.at[z, y, own_rows, pl.ds(0, 256)]),
        load(cgo, WB.at[z, y, own_rows, pl.ds(256, 256)]),
        load(cgi, WB.at[z, y, own_rows, pl.ds(512, 256)]),
    ]
    l_t = [
        load(tok.at[pl.ds(src, n), :], T.at[pl.ds(dst, n), own_cols])
        for dst, n, src in CHUNKS
    ]
    l_small = [load(taps_in, taps_v), load(gain_in, gain_v), load(freq_in, freq_v)]

    barrier = pltpu.get_barrier_semaphore()
    peers = (sib, yp, ym, y2, zp, zm, xp, xm, x2, sp, sm)
    for peer in peers:
        pl.semaphore_signal(barrier, inc=1, device_id=peer, device_id_type=MESH)

    for cp in l_out:
        cp.wait()
    eye = jnp.where(
        lax.broadcasted_iota(jnp.int32, (32, 32), 0)
        == lax.broadcasted_iota(jnp.int32, (32, 32), 1),
        1.0,
        0.0,
    ).astype(BF16)
    WA[z, y, own_rows, 512:768] = nt_dot(eye, owa_v[...]).astype(BF16)
    WB[z, y, own_rows, 768:1024] = nt_dot(eye, owc_v[...]).astype(BF16)

    for cp in l_w:
        cp.wait()
    pl.semaphore_wait(barrier, len(peers))

    sent = []

    def copy(src, dst, rsem, peer, k=0):
        return pltpu.make_async_remote_copy(
            src_ref=src, dst_ref=dst, send_sem=ssem.at[k], recv_sem=rsem,
            device_id=peer, device_id_type=MESH,
        )

    def send(src, dst, rsem, peer, like=None):
        cp = copy(src, dst, rsem, peer, len(sent))
        cp.start()
        sent.append(cp if like is None else like)

    def arrived(ref, rsem):
        copy(ref, ref, rsem, xp).wait_recv()

    ownA = WA.at[z, y, own_rows]
    ownB = WB.at[z, y, own_rows]
    sib_rows = pl.ds(pl.multiple_of((1 - core) * 32, 32), 32)
    sibA = WA.at[z, y, sib_rows]
    sibB = WB.at[z, y, sib_rows]
    send(ownA, ownA, irec.at[0], sib)
    send(ownB, ownB, irec.at[1], sib)

    def cols(d):
        return pl.ds(pl.multiple_of(((x + d) % NX) * QUARTER, QUARTER), QUARTER)

    for i, (dst, n, _) in enumerate(CHUNKS):
        l_t[i].wait()
        blk = T.at[pl.ds(dst, n), own_cols]
        send(blk, blk, xrec.at[i], xp)
        send(blk, blk, xrec.at[4 + i], xm)

    RELAY = (
        ((0, 0, 128, 1),),
        ((1, 128, 128, -1),),
        ((2, 256, 128, 1), (2, 384, 128, -1)),
        ((3, 512, 128, 1), (3, 640, 128, -1)),
    )

    def t_chunk(i, d):
        dst, n, _ = CHUNKS[i]
        return T.at[pl.ds(dst, n), cols(d)]

    def x_relay(i):
        for _, r0, n, direction in RELAY[i]:
            if direction == 1:
                arrived(t_chunk(i, 3), xrec.at[i])
                blk = T.at[pl.ds(r0, n), cols(3)]
                send(blk, blk, xrec.at[8 + r0 // 128], xp, "t")
            else:
                arrived(t_chunk(i, 1), xrec.at[4 + i])
                blk = T.at[pl.ds(r0, n), cols(1)]
                send(blk, blk, xrec.at[8 + r0 // 128], xm, "t")

    def x_rest(i):
        if i == 0:
            arrived(t_chunk(0, 1), xrec.at[4])
            arrived(T.at[pl.ds(0, 128), cols(2)], xrec.at[8])
        elif i == 1:
            arrived(t_chunk(1, 3), xrec.at[1])
            arrived(T.at[pl.ds(128, 128), cols(2)], xrec.at[9])
        else:
            r0 = CHUNKS[i][0]
            arrived(T.at[pl.ds(r0, 128), cols(2)], xrec.at[8 + r0 // 128])
            arrived(T.at[pl.ds(r0 + 128, 128), cols(2)], xrec.at[9 + r0 // 128])

    def rel(dz, dy):
        return (dz % NZ) * NY + dy % NY

    def run_a():
        def piece(dz, dy):
            return WA.at[(z + dz) % NZ, (y + dy) % NY]

        def fwd(dz, dy, peer, ddz, ddy):
            p = piece(dz, dy)
            send(p, p, wrec.at[rel(dz + ddz, dy + ddy)], peer, "a")

        def to_sib(dz, dy):
            p = piece(dz, dy)
            send(p, p, srec.at[rel(dz, dy)], sib, "a")

        def got(dz, dy):
            arrived(piece(dz, dy), wrec.at[rel(dz, dy)])

        arrived(sibA, irec.at[0])
        fwd(0, 0, zp, -1, 0)
        fwd(0, 0, zm, 1, 0)
        fwd(0, 0, yp, 0, -1)
        fwd(0, 0, ym, 0, 1)
        fwd(0, 0, y2, 0, 2)
        for dy in (1, 3, 2):
            got(0, dy)
            fwd(0, dy, zp, -1, 0)
            fwd(0, dy, zm, 1, 0)
            to_sib(0, dy)
        for k in (1, 2, 3):
            for n, dy in enumerate((0, 1, 3, 2)):
                got(-k, dy)
                if k < 3 or n % 2 == 0:
                    fwd(-k, dy, zp, -1, 0)
                to_sib(-k, dy)
                got(k, dy)
                if k < 3 or n % 2 == 1:
                    fwd(k, dy, zm, 1, 0)
                to_sib(k, dy)
            if k == 2:
                x_relay(0)
                x_relay(1)
        x_relay(2)
        for dy in (0, 1, 3, 2):
            got(4, dy)
            to_sib(4, dy)
        x_relay(3)
        arrived(sibB, irec.at[1])
        for r in range(1, 32):
            arrived(WB.at[(z + r // NY) % NZ, (y + r % NY) % NY], srec.at[r])

    def run_b():
        def piece(dz, dy):
            return WB.at[(z + dz) % NZ, (y + dy) % NY]

        def fwd(dz, dy, peer, ddz, ddy):
            p = piece(dz, dy)
            send(p, p, wrec.at[rel(dz + ddz, dy + ddy)], peer, "b")

        def to_sib(dz, dy):
            p = piece(dz, dy)
            send(p, p, srec.at[rel(dz, dy)], sib, "b")

        def got(dz, dy):
            arrived(piece(dz, dy), wrec.at[rel(dz, dy)])

        def z_part(k):
            for dz in ((-k, k) if k < 4 else (4,)):
                got(dz, 0)
                if k < 3 or (k == 3 and dz < 0):
                    fwd(dz, 0, zp if dz < 0 else zm, -1 if dz < 0 else 1, 0)
                fwd(dz, 0, yp, 0, -1)
                fwd(dz, 0, ym, 0, 1)
                to_sib(dz, 0)

        def y_part(k):
            for dz in ((0,) if k == 0 else (-k, k) if k < 4 else (4,)):
                up = k == 0 or (k < 4 and dz > 0)
                got(dz, 3)
                if up:
                    fwd(dz, 3, yp, 0, -1)
                to_sib(dz, 3)
                got(dz, 1)
                if not up:
                    fwd(dz, 1, ym, 0, 1)
                to_sib(dz, 1)

        def d_part(k):
            for dz in ((0,) if k == 0 else (-k, k) if k < 4 else (4,)):
                got(dz, 2)
                to_sib(dz, 2)

        arrived(sibB, irec.at[1])
        fwd(0, 0, zp, -1, 0)
        fwd(0, 0, zm, 1, 0)
        fwd(0, 0, yp, 0, -1)
        fwd(0, 0, ym, 0, 1)
        z_part(1)
        y_part(0)
        z_part(2)
        y_part(1)
        d_part(0)
        z_part(3)
        y_part(2)
        d_part(1)
        x_relay(0)
        x_relay(1)
        z_part(4)
        y_part(3)
        d_part(2)
        y_part(4)
        x_relay(2)
        d_part(3)
        d_part(4)
        x_relay(3)
        arrived(sibA, irec.at[0])
        for r in range(1, 32):
            arrived(WA.at[(z + r // NY) % NZ, (y + r % NY) % NY], srec.at[r])

    for cp in l_small:
        cp.wait()
    lane = lax.broadcasted_iota(jnp.int32, (GRID, HEAD), 1)
    line = lax.broadcasted_iota(jnp.int32, (GRID, HEAD), 0).astype(F32)
    by_row = lane < HEAD // 2
    negative = (lane // 32) % 2 == 0
    freq = freq_v[0:1, :]
    column_angle = line * freq
    column_cos, column_sin = jnp.cos(column_angle), jnp.sin(column_angle)
    first = (s * (ROWS // GRID)).astype(F32)
    row_angle = (lax.broadcasted_iota(jnp.int32, (16, HEAD), 0).astype(F32) + first) * freq
    row_cos, row_sin = jnp.cos(row_angle), jnp.sin(row_angle)
    for r in range(ROWS // GRID):
        COS[r * GRID : (r + 1) * GRID, :] = jnp.where(by_row, row_cos[r : r + 1, :], column_cos)
        sine = jnp.where(by_row, row_sin[r : r + 1, :], column_sin)
        SIN[r * GRID : (r + 1) * GRID, :] = jnp.where(negative, -sine, sine)

    base = len(sent)
    spans = []
    for c, run in ((0, run_a), (1, run_b)):
        @pl.when(core == c)
        def _(run=run):
            run()
            spans.append(sent[base:])
            del sent[base:]
    sent.extend([None] * max(len(span) for span in spans))

    negative = (lax.broadcasted_iota(jnp.int32, (256, HEAD), 1) // 32) % 2 == 0
    row256 = lax.broadcasted_iota(jnp.int32, (256, 1), 0)

    def rotate(u, cosine, sine):
        turned = jnp.where(negative, pltpu.roll(u, 96, 1), pltpu.roll(u, 32, 1))
        return (u * cosine + turned * sine).astype(BF16)

    def weight(ref, c0):
        return ref[:, :, :, c0 : c0 + 256].reshape(WIDTH, 256)

    def project(m):
        rows = slice(256 * m, 256 * m + 256)
        blocks = ORDER[2 * m : 2 * m + 2]
        cosine = jnp.concatenate([COS[b * 128 : b * 128 + 128, :] for b in blocks], 0)
        sine = jnp.concatenate([SIN[b * 128 : b * 128 + 128, :] for b in blocks], 0)
        q = jnp.dot(T[rows, :], weight(WA, 0), preferred_element_type=F32)
        for h in range(2):
            u = rotate(q[:, h * HEAD : (h + 1) * HEAD], cosine, sine)
            for i, b in enumerate(blocks):
                Q[b, h * 128 : (h + 1) * 128, :] = u[i * 128 : (i + 1) * 128]
        kv = jnp.dot(T[rows, :], weight(WA, 256), preferred_element_type=F32)
        k = rotate(kv[:, :HEAD], cosine, sine)
        v = kv[:, HEAD:].astype(BF16)
        for i, b in enumerate(blocks):
            KV[b + 1, :, 0:HEAD] = k[i * 128 : (i + 1) * 128]
            KV[b + 1, :, HEAD:] = v[i * 128 : (i + 1) * 128]
        c_in = jnp.dot(T[rows, :], weight(WB, 0), preferred_element_type=F32)
        before = jnp.dot(T[rows, :], weight(WB, 512), preferred_element_type=F32)
        sec = (before * c_in).astype(BF16)
        for i, b in enumerate(blocks):
            SEC[b] = sec[i * 128 : (i + 1) * 128].astype(F32)
            if m == 0:
                ES[i] = sec[0:16] if i == 0 else sec[240:256]
        after = jnp.dot(T[rows, :], weight(WB, 256), preferred_element_type=F32)
        for i, b in enumerate(blocks):
            GA[b] = after[i * 128 : (i + 1) * 128]

    row128 = lax.broadcasted_iota(jnp.int32, (128, 1), 0)
    taps = taps_v[...].astype(F32)

    def convolve(b):
        sec = SEC[b]
        if b > 0:
            low = SEC[b - 1, 127:128, :]
        else:
            low = jnp.where(s > 0, ER[0].astype(F32)[15:16, :], 0.0)
        if b < 5:
            high = SEC[b + 1, 0:1, :]
        else:
            high = jnp.where(s < NSP - 1, ER[1].astype(F32)[0:1, :], 0.0)
        before = jnp.where(row128 == 0, low, pltpu.roll(sec, 1, 0))
        later = jnp.where(row128 == 127, high, pltpu.roll(sec, 127, 0))
        mix = before * taps[0:1] + sec * taps[1:2] + later * taps[2:3]
        MIX[b * 128 : (b + 1) * 128, 256:512] = (GA[b] * mix).astype(BF16)

    qi = lax.broadcasted_iota(jnp.int32, (256, 384), 0) % 128
    kj = lax.broadcasted_iota(jnp.int32, (256, 384), 1)
    inside = (kj >= qi) & (kj <= qi + 256)
    sink_col = jnp.where(row256 < 128, sink[0], sink[1])

    def attend(b):
        keys = KV[b : b + 3, :, 0:HEAD].reshape(384, HEAD)
        values = KV[b : b + 3, :, HEAD:].reshape(384, HEAD)
        scores = nt_dot(Q[b], keys) * HEAD ** (-0.5)
        valid = inside
        if b == 0:
            valid = valid & ((kj >= 128) | (s > 0))
        if b == 5:
            valid = valid & ((kj < 256) | (s < NSP - 1))
        scores = jnp.where(valid, scores, NEG_BIG)
        top = jnp.maximum(jnp.max(scores, 1, keepdims=True), sink_col)
        w = jnp.exp(scores - top)
        total = jnp.sum(w, 1, keepdims=True) + jnp.exp(sink_col - top)
        probs = (w / total).astype(BF16)
        o = jnp.dot(probs, values, preferred_element_type=F32).astype(BF16)
        rows = slice(b * 128, b * 128 + 128)
        MIX[rows, 0:HEAD] = o[:128]
        MIX[rows, HEAD : 2 * HEAD] = o[128:]

    def halo_send():
        send(KV.at[1], KV.at[7], hrec.at[0], sm)
        send(KV.at[6], KV.at[0], hrec.at[1], sp)
        send(ES.at[0], ER.at[1], hrec.at[2], sm)
        send(ES.at[1], ER.at[0], hrec.at[3], sp)

    def halo_left():
        arrived(KV.at[0], hrec.at[1])
        arrived(ER.at[0], hrec.at[3])

    def halo_right():
        arrived(KV.at[7], hrec.at[0])
        arrived(ER.at[1], hrec.at[2])

    def partial(g, d):
        o = (x + d) % NX
        a = MIX[256 * g : 256 * g + 256, 0:256]
        c = MIX[256 * g : 256 * g + 256, 256:512]
        wa = WA[pl.ds(2 * o, 2), :, :, 512:768].reshape(QUARTER, 256)
        wb = WB[pl.ds(2 * o, 2), :, :, 768:1024].reshape(QUARTER, 256)
        return nt_dot(a, wa) + nt_dot(c, wb)

    def spread_out(g):
        p = partial(g, 2).astype(BF16)
        S2[g, 0] = p[:128]
        S2[g, 1] = p[128:]
        send(S2.at[g, 0], R2.at[g, 0], r2rec.at[2 * g], xp)
        send(S2.at[g, 1], R2.at[g, 1], r2rec.at[2 * g + 1], xm)
        p = partial(g, 1)
        PT[g] = p[:128]
        S1[g, 0, 1] = p[128:].astype(BF16)
        send(S1.at[g, 0, 1], R1.at[g, 0, 1], r1rec.at[4 * g + 1], xp)
        p = partial(g, 3)
        PB[g] = p[128:]
        S1[g, 1, 0] = p[:128].astype(BF16)
        send(S1.at[g, 1, 0], R1.at[g, 1, 0], r1rec.at[4 * g + 2], xm)
        PX[g] = partial(g, 0)

    def sum_relay(g):
        arrived(R2.at[g, 0], r2rec.at[2 * g])
        S1[g, 0, 0] = (PT[g] + R2[g, 0].astype(F32)).astype(BF16)
        send(S1.at[g, 0, 0], R1.at[g, 0, 0], r1rec.at[4 * g], xp)
        arrived(R2.at[g, 1], r2rec.at[2 * g + 1])
        S1[g, 1, 1] = (PB[g] + R2[g, 1].astype(F32)).astype(BF16)
        send(S1.at[g, 1, 1], R1.at[g, 1, 1], r1rec.at[4 * g + 3], xm)

    def local_stats(g):
        for i in range(2):
            for half in range(2):
                arrived(R1.at[g, i, half], r1rec.at[4 * g + 2 * i + half])
        for half in range(2):
            rows = slice(128 * half, 128 * half + 128)
            t = PX[g, rows, :] + R1[g, 0, half].astype(F32) + R1[g, 1, half].astype(F32)
            PX[g, rows, :] = t
            mean = jnp.sum(t, 1, keepdims=True) * (1.0 / QUARTER)
            m2 = jnp.sum(jnp.square(t - mean), 1, keepdims=True)
            lane = lax.broadcasted_iota(jnp.int32, (128, 128), 1)
            both = jnp.where(lane == 0, mean, m2)
            ST[g, 0, half] = jnp.transpose(both)[0:8, :]
        for d, peer, slot in ((1, xp, 3), (3, xm, 1), (2, x2, 2)):
            send(ST.at[g, 0], ST.at[g, slot], strec.at[3 * g + slot - 1], peer)

    def finish(g):
        for slot in (1, 2, 3):
            arrived(ST.at[g, slot], strec.at[3 * g + slot - 1])
        for half in range(2):
            rows = slice(128 * half, 128 * half + 128)
            parts = [ST[g, slot, half] for slot in range(4)]
            means = [p[0:1, :] for p in parts]
            mean = (means[0] + means[1] + means[2] + means[3]) * 0.25
            m2 = sum(p[1:2, :] for p in parts)
            for m in means:
                m2 = m2 + QUARTER * jnp.square(m - mean)
            scale = lax.rsqrt(m2 * (1.0 / WIDTH) + EPS)
            line = lax.broadcasted_iota(jnp.int32, (128, 128), 0)
            columns = jnp.transpose(jnp.where(line == 0, mean, scale))
            normed = (PX[g, rows, :] - columns[:, 0:1]) * columns[:, 1:2] * gain_v[0:1, :]
            OUT[g, rows, :] = normed.astype(BF16)
        cp = pltpu.make_async_copy(OUT.at[g], out.at[pl.ds(256 * g, 256), :], osem.at[g])
        cp.start()
        outs.append(cp)

    outs = []
    x_rest(0)
    x_rest(1)
    project(0)
    halo_send()
    x_rest(2)
    project(1)
    convolve(1)
    attend(1)
    halo_left()
    convolve(0)
    attend(0)
    spread_out(0)
    x_rest(3)
    project(2)
    convolve(2)
    convolve(3)
    attend(2)
    attend(3)
    spread_out(1)
    sum_relay(0)
    convolve(4)
    attend(4)
    halo_right()
    convolve(5)
    attend(5)
    spread_out(2)
    sum_relay(1)
    local_stats(0)
    sum_relay(2)
    finish(0)
    local_stats(1)
    finish(1)
    local_stats(2)
    finish(2)
    for cp in sent:
        if cp is not None:
            cp.wait_send()
    likes = {"a": WA.at[0, 0], "b": WB.at[0, 0], "t": T.at[pl.ds(0, 128), pl.ds(0, QUARTER)]}
    for c, span in enumerate(spans):
        @pl.when(core == c)
        def _(span=span):
            for i, like in enumerate(span):
                copy(likes[like], likes[like], osem.at[0], xp, base + i).wait_send()
    for cp in outs:
        cp.wait()


def body(
    tokens, query_weight, key_projection, value_projection, conv_in_weight, conv_gate_out,
    conv_gate_in, conv_taps, head_sink_logit, out_attn_weight, out_conv_weight, out_gain,
):
    half = HEAD // 2
    inverse = np.float32(THETA) ** (-np.arange(0, half, 2, dtype=np.float32) / np.float32(half))
    freq = jnp.asarray(np.tile(inverse.astype(np.float32), 4)[None, :])
    anywhere = pl.BlockSpec(memory_space=pl.ANY)
    specs = [anywhere] * 13
    specs[8] = pl.BlockSpec(memory_space=pltpu.SMEM)
    dma = pltpu.SemaphoreType.DMA
    return pl.pallas_call(
        kernel,
        out_shape=jax.ShapeDtypeStruct((ROWS, QUARTER), BF16),
        in_specs=specs,
        out_specs=anywhere,
        scratch_shapes=[
            pltpu.VMEM((ROWS, WIDTH), BF16),
            pltpu.VMEM((NZ, NY, 64, CA), BF16),
            pltpu.VMEM((NZ, NY, 64, CB), BF16),
            pltpu.VMEM((8, 128, 256), BF16),
            pltpu.VMEM((6, 256, 128), BF16),
            pltpu.VMEM((6, 128, 256), F32),
            pltpu.VMEM((6, 128, 256), F32),
            pltpu.VMEM((ROWS, QUARTER), BF16),
            pltpu.VMEM((2, 16, 256), BF16),
            pltpu.VMEM((2, 16, 256), BF16),
            pltpu.VMEM((ROWS, HEAD), F32),
            pltpu.VMEM((ROWS, HEAD), F32),
            pltpu.VMEM((3, 2, 128, QUARTER), BF16),
            pltpu.VMEM((3, 128, QUARTER), F32),
            pltpu.VMEM((3, 128, QUARTER), F32),
            pltpu.VMEM((3, 256, QUARTER), F32),
            pltpu.VMEM((3, 2, 2, 128, QUARTER), BF16),
            pltpu.VMEM((3, 2, 128, QUARTER), BF16),
            pltpu.VMEM((3, 2, 2, 128, QUARTER), BF16),
            pltpu.VMEM((3, 4, 2, 8, 128), F32),
            pltpu.VMEM((3, 256, QUARTER), BF16),
            pltpu.VMEM((256, 32), BF16),
            pltpu.VMEM((256, 32), BF16),
            pltpu.VMEM((3, 256), BF16),
            pltpu.VMEM((1, QUARTER), F32),
            pltpu.VMEM((1, HEAD), F32),
            dma((16,)),
            dma((144,)),
            dma((32,)),
            dma((32,)),
            dma((2,)),
            dma((14,)),
            dma((4,)),
            dma((6,)),
            dma((12,)),
            dma((9,)),
            dma((3,)),
        ],
        compiler_params=pltpu.CompilerParams(
            collective_id=0, has_side_effects=True, vmem_limit_bytes=56 * 1024 * 1024
        ),
    )(
        tokens, query_weight, key_projection, value_projection, conv_in_weight, conv_gate_out,
        conv_gate_in, conv_taps, head_sink_logit, out_attn_weight, out_conv_weight,
        out_gain.reshape(1, -1), freq,
    )


def solution(mesh):
    return jax.shard_map(
        body,
        mesh=mesh,
        in_specs=(
            P("sp", "tp"),
            P("sp", "tp"),
            P("sp", "tp"),
            P("sp", "tp"),
            P("sp", "tp"),
            P("sp", "tp"),
            P("sp", "tp"),
            P(None, "tp"),
            P("tp"),
            P("tp", "sp"),
            P("tp", "sp"),
            P("tp"),
        ),
        out_specs=P("sp", "tp"),
        check_vma=False,
    )
```

time: 208 us -> 84.6 us (0.41); the launches traced: 204 us -> 84.4 us
  Pallas kernels: 0 us -> 80.2 us
  waiting for transfers between devices: 72.6 us -> 0 us
  blocking collectives: 50.4 us -> 0 us
  starting transfers between devices: 27.6 us -> 0 us
  between operations: 13.8 us -> 0.01 us
  matrix products: 13.7 us -> 0 us
  local copies, waits for them, and re-layouts: 16.1 us -> 4.26 us
  other arithmetic: 10.1 us -> 0 us
    pallas_call x0 -> x1, Pallas kernels: none -> 80.2 us  [body(): pl.pallas_call(kernel, out_shape=jax.ShapeDtypeStruct((ROWS, QUARTER), BF...]
    all_to_all x2 -> x0, blocking collectives: 50.4 us -> none  [the longest x1 42.6 us: sum_at_owner(): lax.all_to_all(blocks, axis, split_axis=0, concat_axis=0, tiled=True)]
    all_gather x1 -> x0, waiting for transfers between devices: 40.7 us -> none  [sent_together(): lax.all_gather(both, axis, axis=dim, tiled=True)]
    all_to_all x2 -> x0, waiting for transfers between devices: 31.9 us -> none  [copy_for_each(): return lax.all_to_all(copies, axis, split_axis=0, concat_axis=0, tiled=True)]
    all_to_all x2 -> x0, starting transfers between devices: 18.4 us -> none  [copy_for_each(): return lax.all_to_all(copies, axis, split_axis=0, concat_axis=0, tiled=True)]
    dot_general x9 -> x0, matrix products: 13.7 us -> none  [the longest x6 8.89 us: body(): jnp.dot(whole, piece, preferred_element_type=jnp.float32)]
    ppermute x4 -> x0, starting transfers between devices: 9.14 us -> none  [the longest x2 6.4 us: with_halo(): lax.ppermute(lax.slice_in_dim(block, block.shape[dim] - width, None, axis...]
    broadcast_in_dim x3 -> x0, local copies, waits for them, and re-layouts: 3.53 us -> none  [copy_for_each(): copies = jnp.broadcast_to(array, (lax.axis_size(axis), *array.shape))]
  transfers between devices with their start and end apart: 7 -> 0, of which waited for: 2 -> 0; matrix products, arithmetic and copies ran while one was open for 14% -> 0% of each run, Pallas kernels for 0% -> 0%
where the time goes in v1:
time: 84.6 us; the launch traced here: 84.4 us
  Pallas kernels  80.2 us (95%)
  local copies, waits for them, and re-layouts  4.26 us (5%)
    pallas_call x1, Pallas kernels, body(): pl.pallas_call(kernel, out_shape=jax.ShapeDtypeStruct((ROWS, QUARTER), BF...  80.2 us
    unnamed x5, local copies, waits for them, and re-layouts  4.26 us

profile of v1, /device:TPU:2, one launch (start us, length us, event | category | flops | bytes accessed | tf_op | source)
XLA Modules:
  0.0 84.4 jit_solution(8848449500091443099)
XLA Ops:
  0.0 0.0 copy-start
  0.0 1.5 %copy.14.owa = bf16[256,32]{1,0:T(8,128)(2,1)} copy(bf16[256,32]{0,1:T(8,128)(2,1)} %param.22) | data formatting | bytes 32768 | tf_op args[9]
  1.5 0.0 copy-done
  1.5 0.7 copy.15.owc
  2.2 80.2 %shard_map.127 = bf16[768,512]{1,0:T(8,128)(2,1)} custom-call(bf16[768,512]{1,0:T(8,128)(2,1)} %tok.1, bf16[32,256]{1,0:T(8,128)(2,1)} %qw.1, bf16[32,128]{1,0:T(8,128)(2,1)} %kw.1, bf16[32,128]{1,0:T(8,128)(2,1)} %vw.1, bf16[32,256]{1,0:T(8,128)(2,1)} %cin.1, bf16[32,256]{1,0:T(8,128)(2,1)} %cgo.1, bf16[32,256]{1,0:T(8,128)(2,1)} %cgi.1, ...), custom_call_target="tpu_custom_call" | custom-call | tf_op jit(solution)/shard_map/pallas_call | solution.py:536
  82.4 2.1 %copy.17 = bf16[768,512]{1,0:T(8,128)(2,1)} copy(bf16[768,512]{1,0:T(8,128)(2,1)} %shard_map.127) | data formatting | bytes 1572864
Async XLA Ops:
  0.0 1.5 %copy-start = (bf16[256,32]{0,1:T(8,128)(2,1)S(1)}, bf16[256,32]{0,1:T(8,128)(2,1)}, u32[]{:S(2)}) copy-start(bf16[256,32]{0,1:T(8,128)(2,1)} %param.23) | copy-start | bytes 49156

commit v2 on v1

v2 whole, which is shorter than its diff:
```python
import functools

import jax
import jax.numpy as jnp
import numpy as np
from jax import lax
from jax.experimental import pallas as pl
from jax.experimental.pallas import tpu as pltpu
from jax.sharding import PartitionSpec as P

MESH = pl.DeviceIdType.MESH
F32 = jnp.float32
BF16 = jnp.bfloat16

HEAD = 128
WINDOW = 128
GRID = 64
NEG_BIG = -1e30
THETA = 10000.0
EPS = 1e-05

NZ, NY, NX, NSP = 8, 4, 4, 64
ROWS = 768
WIDTH = 2048
QUARTER = 512
ORDER = (0, 5, 1, 2, 3, 4)
CHUNKS = ((0, 128, 0), (128, 128, 640), (256, 256, 128), (512, 256, 384))


def nt_dot(a, b):
    return lax.dot_general(a, b, (((1,), (1,)), ((), ())), preferred_element_type=F32)


def kernel(
    tok, qw, kw, vw, cin, cgo, cgi, taps_in, sink, owa, owc, gain_in, freq_in, out,
    T, WA, WB, WC, WD, KV, Q, SEC, GA, MIX, ES, ER, COS, SIN, S2, PT, PB, PX, S1, R2, R1, ST, OUT,
    taps_v, gain_v, freq_v,
    lsem, met, csem, wsem, wrec, srec, irec, xrec, hrec, r2rec, r1rec, strec, osem,
):
    s = lax.axis_index("sp")
    x = lax.axis_index("tp")
    core = s % 2
    chip = s // 2
    y = chip % NY
    z = chip // NY

    def at(zz, yy, cc):
        return ((zz % NZ) * NY + yy % NY) * 2 + cc

    sib = (at(z, y, 1 - core), x)
    yp, ym, y2 = [(at(z, y + d, core), x) for d in (1, 3, 2)]
    zp, zm = [(at(z + d, y, core), x) for d in (1, NZ - 1)]
    xp, xm, x2 = [(s, (x + d) % NX) for d in (1, 3, 2)]
    sp, sm = [((s + d) % NSP, x) for d in (1, NSP - 1)]

    loads = []

    def load(src, dst):
        cp = pltpu.make_async_copy(src, dst, lsem.at[len(loads)])
        cp.start()
        loads.append(cp)
        return cp

    own_cols = pl.ds(pl.multiple_of(x * QUARTER, QUARTER), QUARTER)
    own_rows = pl.ds(pl.multiple_of(core * 32, 32), 32)
    l_w = [
        load(qw, WA.at[z, y, own_rows, pl.ds(0, 256)]),
        load(kw, WA.at[z, y, own_rows, pl.ds(256, 128)]),
        load(vw, WA.at[z, y, own_rows, pl.ds(384, 128)]),
        load(cin, WB.at[z, y, own_rows, pl.ds(0, 256)]),
        load(cgi, WB.at[z, y, own_rows, pl.ds(256, 256)]),
        load(owa, WC.at[z, y, own_rows]),
        load(cgo, WD.at[z, y, own_rows, pl.ds(0, 256)]),
        load(owc, WD.at[z, y, own_rows, pl.ds(256, 256)]),
    ]
    l_t = [
        load(tok.at[pl.ds(src, n), :], T.at[pl.ds(dst, n), own_cols])
        for dst, n, src in CHUNKS
    ]
    l_small = [load(taps_in, taps_v), load(gain_in, gain_v), load(freq_in, freq_v)]

    barrier = pltpu.get_barrier_semaphore()

    def greet(peer):
        pl.semaphore_signal(barrier, inc=1, device_id=peer, device_id_type=MESH)

    greet(sib)
    for d in (1, 3):
        greet((at(z, y, 0), (x + d) % NX))
        greet((at(z, y + d, 1), x))
    for d in (1, NZ - 1):
        greet((at(z + d, y, 1), x))

    @pl.when(core == 0)
    def _():
        greet((at(z, y + 2, 1), x))

    for cp in l_w:
        cp.wait()

    @pl.when(core == 0)
    def _():
        pl.semaphore_wait(barrier, 5)
        pl.semaphore_signal(met, inc=1, device_id=sib, device_id_type=MESH)

    @pl.when(core == 1)
    def _():
        pl.semaphore_wait(met, 1)

    counts = [0, 0, 0, 0]

    def copy(src, dst, rsem, peer, ssem):
        return pltpu.make_async_remote_copy(
            src_ref=src, dst_ref=dst, send_sem=ssem, recv_sem=rsem,
            device_id=peer, device_id_type=MESH,
        )

    def send(src, dst, rsem, peer, ssem):
        copy(src, dst, rsem, peer, ssem).start()

    def send_weights(n, src, rsem, peer):
        i = counts[n]
        counts[n] += 1
        send(src, src, rsem, peer, wsem.at[n // 2, 0 if i < 32 else 1 if i < 60 else 2])

    def sent(ref, ssem):
        copy(ref, ref, osem.at[0], xp, ssem).wait_send()

    def on_core(c, *steps):
        @pl.when(core == c)
        def _():
            for step, *args in steps:
                step(*args)

    def arrived(ref, rsem):
        copy(ref, ref, rsem, xp, csem.at[0]).wait_recv()

    sib_rows = pl.ds(pl.multiple_of((1 - core) * 32, 32), 32)
    W = (WA, WB, WC, WD)
    for n, w in enumerate(W):
        send(w.at[z, y, own_rows], w.at[z, y, own_rows], irec.at[n], sib, csem.at[n])

    def from_sib(n):
        arrived(W[n].at[z, y, sib_rows], irec.at[n])

    def cols(d):
        return pl.ds(pl.multiple_of(((x + d) % NX) * QUARTER, QUARTER), QUARTER)

    def x_send(i):
        dst, n, _ = CHUNKS[i]
        blk = T.at[pl.ds(dst, n), own_cols]
        send(blk, blk, xrec.at[i], xp, csem.at[4])
        send(blk, blk, xrec.at[4 + i], xm, csem.at[4])

    for cp in l_t:
        cp.wait()
    for i in range(3):
        x_send(i)

    @pl.when(core == 1)
    def _():
        pl.semaphore_wait(barrier, 10)
        pl.semaphore_signal(met, inc=1, device_id=sib, device_id_type=MESH)

    @pl.when(core == 0)
    def _():
        pl.semaphore_wait(met, 1)

    RELAY = (
        ((0, 0, 128, 1),),
        ((1, 128, 128, -1),),
        ((2, 256, 128, 1), (2, 384, 128, -1)),
        ((3, 512, 128, 1), (3, 640, 128, -1)),
    )

    def t_chunk(i, d):
        dst, n, _ = CHUNKS[i]
        return T.at[pl.ds(dst, n), cols(d)]

    def x_relay(i):
        for _, r0, n, direction in RELAY[i]:
            if direction == 1:
                arrived(t_chunk(i, 3), xrec.at[i])
                blk = T.at[pl.ds(r0, n), cols(3)]
                send(blk, blk, xrec.at[8 + r0 // 128], xp, csem.at[4])
            else:
                arrived(t_chunk(i, 1), xrec.at[4 + i])
                blk = T.at[pl.ds(r0, n), cols(1)]
                send(blk, blk, xrec.at[8 + r0 // 128], xm, csem.at[4])

    def x_rest(i):
        if i == 0:
            arrived(t_chunk(0, 1), xrec.at[4])
            arrived(T.at[pl.ds(0, 128), cols(2)], xrec.at[8])
        elif i == 1:
            arrived(t_chunk(1, 3), xrec.at[1])
            arrived(T.at[pl.ds(128, 128), cols(2)], xrec.at[9])
        else:
            r0 = CHUNKS[i][0]
            arrived(T.at[pl.ds(r0, 128), cols(2)], xrec.at[8 + r0 // 128])
            arrived(T.at[pl.ds(r0 + 128, 128), cols(2)], xrec.at[9 + r0 // 128])

    def rel(dz, dy):
        return (dz % NZ) * NY + dy % NY

    def piece(n, dz, dy):
        return W[n].at[(z + dz) % NZ, (y + dy) % NY]

    def fwd(n, dz, dy, peer, ddz, ddy):
        p = piece(n, dz, dy)
        send_weights(n, p, wrec.at[n // 2, rel(dz + ddz, dy + ddy)], peer)

    def to_sib(n, dz, dy):
        p = piece(n, dz, dy)
        send_weights(n, p, srec.at[n // 2, 1 if dz == 0 else 0], sib)

    def got(n, dz, dy):
        arrived(piece(n, dz, dy), wrec.at[n // 2, rel(dz, dy)])

    def all_from_sib(n):
        from_sib(n)
        arrived(W[n].at[pl.ds(0, 7)], srec.at[n // 2, 0])
        arrived(W[n].at[0, pl.ds(0, 3)], srec.at[n // 2, 1])

    def a_ysend(n):
        from_sib(n)
        fwd(n, 0, 0, yp, 0, -1)
        fwd(n, 0, 0, ym, 0, 1)
        fwd(n, 0, 0, y2, 0, 2)

    def a_zsend(n):
        fwd(n, 0, 0, zp, -1, 0)
        fwd(n, 0, 0, zm, 1, 0)

    def a_y(n):
        for dy in (1, 3, 2):
            got(n, 0, dy)
            fwd(n, 0, dy, zp, -1, 0)
            fwd(n, 0, dy, zm, 1, 0)
            to_sib(n, 0, dy)

    def a_hop(n, k):
        for i, dy in enumerate((0, 1, 3, 2)):
            for dz in (-k, k) if k < 4 else (4,):
                got(n, dz, dy)
                if dz < 0 and (k < 3 or i % 2 == 0):
                    fwd(n, dz, dy, zp, -1, 0)
                if 0 < dz < 4 and (k < 3 or i % 2 == 1):
                    fwd(n, dz, dy, zm, 1, 0)
                to_sib(n, dz, dy)

    def ring(k):
        return (0,) if k == 0 else (-k, k) if k < 4 else (4,)

    def b_start(n):
        from_sib(n)
        fwd(n, 0, 0, zp, -1, 0)
        fwd(n, 0, 0, zm, 1, 0)

    def b_z(n, k):
        for dz in ring(k):
            got(n, dz, 0)
            if dz < 0:
                fwd(n, dz, 0, zp, -1, 0)
            elif k < 3:
                fwd(n, dz, 0, zm, 1, 0)
            to_sib(n, dz, 0)

    def b_zy(n, k):
        for dz in ring(k):
            fwd(n, dz, 0, yp, 0, -1)
            fwd(n, dz, 0, ym, 0, 1)

    def b_y(n, k):
        for dz in ring(k):
            up = k == 0 or 0 < dz < 4
            got(n, dz, 3)
            if up:
                fwd(n, dz, 3, yp, 0, -1)
            to_sib(n, dz, 3)
            got(n, dz, 1)
            if not up:
                fwd(n, dz, 1, ym, 0, 1)
            to_sib(n, dz, 1)

    def b_d(n, k):
        for dz in ring(k):
            got(n, dz, 2)
            to_sib(n, dz, 2)

    for cp in l_small:
        cp.wait()
    lane = lax.broadcasted_iota(jnp.int32, (GRID, HEAD), 1)
    line = lax.broadcasted_iota(jnp.int32, (GRID, HEAD), 0).astype(F32)
    by_row = lane < HEAD // 2
    negative = (lane // 32) % 2 == 0
    freq = freq_v[0:1, :]
    column_angle = line * freq
    column_cos, column_sin = jnp.cos(column_angle), jnp.sin(column_angle)
    first = (s * (ROWS // GRID)).astype(F32)
    row_angle = (lax.broadcasted_iota(jnp.int32, (16, HEAD), 0).astype(F32) + first) * freq
    row_cos, row_sin = jnp.cos(row_angle), jnp.sin(row_angle)
    for r in range(ROWS // GRID):
        COS[r * GRID : (r + 1) * GRID, :] = jnp.where(by_row, row_cos[r : r + 1, :], column_cos)
        sine = jnp.where(by_row, row_sin[r : r + 1, :], column_sin)
        SIN[r * GRID : (r + 1) * GRID, :] = jnp.where(negative, -sine, sine)

    negative = (lax.broadcasted_iota(jnp.int32, (256, HEAD), 1) // 32) % 2 == 0
    row256 = lax.broadcasted_iota(jnp.int32, (256, 1), 0)

    def rotate(u, cosine, sine):
        turned = jnp.where(negative, pltpu.roll(u, 96, 1), pltpu.roll(u, 32, 1))
        return (u * cosine + turned * sine).astype(BF16)

    def weight(ref, c0):
        return ref[:, :, :, c0 : c0 + 256].reshape(WIDTH, 256)

    def project(m):
        rows = slice(256 * m, 256 * m + 256)
        blocks = ORDER[2 * m : 2 * m + 2]
        cosine = jnp.concatenate([COS[b * 128 : b * 128 + 128, :] for b in blocks], 0)
        sine = jnp.concatenate([SIN[b * 128 : b * 128 + 128, :] for b in blocks], 0)
        q = jnp.dot(T[rows, :], weight(WA, 0), preferred_element_type=F32)
        for h in range(2):
            u = rotate(q[:, h * HEAD : (h + 1) * HEAD], cosine, sine)
            for i, b in enumerate(blocks):
                Q[b, h * 128 : (h + 1) * 128, :] = u[i * 128 : (i + 1) * 128]
        kv = jnp.dot(T[rows, :], weight(WA, 256), preferred_element_type=F32)
        k = rotate(kv[:, :HEAD], cosine, sine)
        v = kv[:, HEAD:].astype(BF16)
        for i, b in enumerate(blocks):
            KV[b + 1, :, 0:HEAD] = k[i * 128 : (i + 1) * 128]
            KV[b + 1, :, HEAD:] = v[i * 128 : (i + 1) * 128]

    def project_conv(m):
        rows = slice(256 * m, 256 * m + 256)
        blocks = ORDER[2 * m : 2 * m + 2]
        c_in = jnp.dot(T[rows, :], weight(WB, 0), preferred_element_type=F32)
        before = jnp.dot(T[rows, :], weight(WB, 256), preferred_element_type=F32)
        sec = (before * c_in).astype(BF16)
        for i, b in enumerate(blocks):
            SEC[b] = sec[i * 128 : (i + 1) * 128].astype(F32)
            if m == 0:
                ES[i] = sec[0:16] if i == 0 else sec[240:256]
        after = jnp.dot(T[rows, :], weight(WD, 0), preferred_element_type=F32)
        for i, b in enumerate(blocks):
            GA[b] = after[i * 128 : (i + 1) * 128]

    row128 = lax.broadcasted_iota(jnp.int32, (128, 1), 0)
    taps = taps_v[...].astype(F32)

    def convolve(b):
        sec = SEC[b]
        if b > 0:
            low = SEC[b - 1, 127:128, :]
        else:
            low = jnp.where(s > 0, ER[0].astype(F32)[15:16, :], 0.0)
        if b < 5:
            high = SEC[b + 1, 0:1, :]
        else:
            high = jnp.where(s < NSP - 1, ER[1].astype(F32)[0:1, :], 0.0)
        before = jnp.where(row128 == 0, low, pltpu.roll(sec, 1, 0))
        later = jnp.where(row128 == 127, high, pltpu.roll(sec, 127, 0))
        mix = before * taps[0:1] + sec * taps[1:2] + later * taps[2:3]
        MIX[b * 128 : (b + 1) * 128, 256:512] = (GA[b] * mix).astype(BF16)

    qi = lax.broadcasted_iota(jnp.int32, (256, 384), 0) % 128
    kj = lax.broadcasted_iota(jnp.int32, (256, 384), 1)
    inside = (kj >= qi) & (kj <= qi + 256)
    sink_col = jnp.where(row256 < 128, sink[0], sink[1])

    def attend(b):
        keys = KV[b : b + 3, :, 0:HEAD].reshape(384, HEAD)
        values = KV[b : b + 3, :, HEAD:].reshape(384, HEAD)
        scores = nt_dot(Q[b], keys) * HEAD ** (-0.5)
        valid = inside
        if b == 0:
            valid = valid & ((kj >= 128) | (s > 0))
        if b == 5:
            valid = valid & ((kj < 256) | (s < NSP - 1))
        scores = jnp.where(valid, scores, NEG_BIG)
        top = jnp.maximum(jnp.max(scores, 1, keepdims=True), sink_col)
        w = jnp.exp(scores - top)
        total = jnp.sum(w, 1, keepdims=True) + jnp.exp(sink_col - top)
        probs = (w / total).astype(BF16)
        o = jnp.dot(probs, values, preferred_element_type=F32).astype(BF16)
        rows = slice(b * 128, b * 128 + 128)
        MIX[rows, 0:HEAD] = o[:128]
        MIX[rows, HEAD : 2 * HEAD] = o[128:]

    def halo_send():
        send(KV.at[1], KV.at[7], hrec.at[0], sm, csem.at[5])
        send(KV.at[6], KV.at[0], hrec.at[1], sp, csem.at[5])

    def edge_send():
        send(ES.at[0], ER.at[1], hrec.at[2], sm, csem.at[6])
        send(ES.at[1], ER.at[0], hrec.at[3], sp, csem.at[6])

    def halo_left():
        arrived(KV.at[0], hrec.at[1])

    def edge_left():
        arrived(ER.at[0], hrec.at[3])

    def halo_right():
        arrived(KV.at[7], hrec.at[0])
        arrived(ER.at[1], hrec.at[2])

    def partial(g, d):
        o = (x + d) % NX
        a = MIX[256 * g : 256 * g + 256, 0:256]
        c = MIX[256 * g : 256 * g + 256, 256:512]
        wa = WC[pl.ds(2 * o, 2)].reshape(QUARTER, 256)
        wb = WD[pl.ds(2 * o, 2), :, :, 256:512].reshape(QUARTER, 256)
        return nt_dot(a, wa) + nt_dot(c, wb)

    def spread_out(g):
        p = partial(g, 2).astype(BF16)
        S2[g, 0] = p[:128]
        S2[g, 1] = p[128:]
        send(S2.at[g, 0], R2.at[g, 0], r2rec.at[2 * g], xp, csem.at[7])
        send(S2.at[g, 1], R2.at[g, 1], r2rec.at[2 * g + 1], xm, csem.at[7])
        p = partial(g, 1)
        PT[g] = p[:128]
        S1[g, 0, 1] = p[128:].astype(BF16)
        send(S1.at[g, 0, 1], R1.at[g, 0, 1], r1rec.at[g], xp, csem.at[8])
        p = partial(g, 3)
        PB[g] = p[128:]
        S1[g, 1, 0] = p[:128].astype(BF16)
        send(S1.at[g, 1, 0], R1.at[g, 1, 0], r1rec.at[g], xm, csem.at[8])
        PX[g] = partial(g, 0)

    def sum_relay(g):
        arrived(R2.at[g, 0], r2rec.at[2 * g])
        S1[g, 0, 0] = (PT[g] + R2[g, 0].astype(F32)).astype(BF16)
        send(S1.at[g, 0, 0], R1.at[g, 0, 0], r1rec.at[g], xp, csem.at[8])
        arrived(R2.at[g, 1], r2rec.at[2 * g + 1])
        S1[g, 1, 1] = (PB[g] + R2[g, 1].astype(F32)).astype(BF16)
        send(S1.at[g, 1, 1], R1.at[g, 1, 1], r1rec.at[g], xm, csem.at[8])

    def local_stats(g):
        arrived(R1.at[g], r1rec.at[g])
        for half in range(2):
            rows = slice(128 * half, 128 * half + 128)
            t = PX[g, rows, :] + R1[g, 0, half].astype(F32) + R1[g, 1, half].astype(F32)
            PX[g, rows, :] = t
            mean = jnp.sum(t, 1, keepdims=True) * (1.0 / QUARTER)
            m2 = jnp.sum(jnp.square(t - mean), 1, keepdims=True)
            lane = lax.broadcasted_iota(jnp.int32, (128, 128), 1)
            both = jnp.where(lane == 0, mean, m2)
            ST[g, 0, half] = jnp.transpose(both)[0:8, :]
        for d, peer, slot in ((1, xp, 3), (3, xm, 1), (2, x2, 2)):
            send(ST.at[g, 0], ST.at[g, slot], strec.at[g], peer, csem.at[9])

    def finish(g):
        arrived(ST.at[g, pl.ds(1, 3)], strec.at[g])
        for half in range(2):
            rows = slice(128 * half, 128 * half + 128)
            parts = [ST[g, slot, half] for slot in range(4)]
            means = [p[0:1, :] for p in parts]
            mean = (means[0] + means[1] + means[2] + means[3]) * 0.25
            m2 = sum(p[1:2, :] for p in parts)
            for m in means:
                m2 = m2 + QUARTER * jnp.square(m - mean)
            scale = lax.rsqrt(m2 * (1.0 / WIDTH) + EPS)
            line = lax.broadcasted_iota(jnp.int32, (128, 128), 0)
            columns = jnp.transpose(jnp.where(line == 0, mean, scale))
            normed = (PX[g, rows, :] - columns[:, 0:1]) * columns[:, 1:2] * gain_v[0:1, :]
            OUT[g, rows, :] = normed.astype(BF16)
        cp = pltpu.make_async_copy(OUT.at[g], out.at[pl.ds(256 * g, 256), :], osem.at[g])
        cp.start()
        outs.append(cp)

    outs = []
    on_core(
        0,
        (a_ysend, 0), (a_zsend, 0), (a_ysend, 2), (a_zsend, 2), (a_y, 0), (a_hop, 0, 1),
        (x_relay, 0), (x_relay, 1), (x_send, 3),
        (a_y, 2), (a_hop, 0, 2), (a_hop, 2, 1), (x_relay, 2),
        (a_hop, 0, 3), (a_hop, 2, 2), (a_hop, 0, 4), (x_relay, 3),
    )
    on_core(
        1,
        (b_start, 1), (b_zy, 1, 0), (b_start, 3),
        (b_z, 1, 1), (b_zy, 1, 1), (b_zy, 3, 0), (b_z, 3, 1), (b_zy, 3, 1),
        (b_z, 1, 2), (b_zy, 1, 2), (b_y, 1, 0), (b_z, 3, 2), (b_zy, 3, 2), (b_y, 3, 0), (b_y, 1, 1),
        (x_relay, 0), (x_relay, 1), (x_send, 3),
        (b_z, 1, 3), (b_zy, 1, 3), (b_y, 3, 1), (b_z, 3, 3), (b_zy, 3, 3),
        (b_d, 1, 0), (b_d, 3, 0), (b_y, 1, 2), (b_d, 1, 1), (b_y, 3, 2),
        (b_z, 1, 4), (b_zy, 1, 4), (b_d, 3, 1), (b_z, 3, 4), (b_zy, 3, 4),
        (x_relay, 2), (b_y, 1, 3), (b_y, 3, 3), (b_d, 1, 2), (b_d, 3, 2), (b_y, 1, 4), (b_y, 3, 4),
        (x_relay, 3), (all_from_sib, 0),
    )
    x_rest(0)
    x_rest(1)
    project(0)
    halo_send()
    on_core(0, (a_hop, 2, 3))
    on_core(1, (b_d, 1, 3), (b_d, 3, 3))
    x_rest(2)
    project(1)
    on_core(0, (a_hop, 2, 4))
    on_core(1, (b_d, 1, 4), (b_d, 3, 4))
    attend(1)
    halo_left()
    attend(0)
    on_core(0, (all_from_sib, 1), (all_from_sib, 3))
    on_core(1, (all_from_sib, 2))
    project_conv(0)
    edge_send()
    project_conv(1)
    convolve(1)
    edge_left()
    convolve(0)
    spread_out(0)
    x_rest(3)
    project(2)
    project_conv(2)
    convolve(2)
    convolve(3)
    attend(2)
    attend(3)
    spread_out(1)
    sum_relay(0)
    convolve(4)
    attend(4)
    halo_right()
    convolve(5)
    attend(5)
    spread_out(2)
    sum_relay(1)
    local_stats(0)
    sum_relay(2)
    local_stats(1)
    local_stats(2)
    finish(0)
    finish(1)
    finish(2)
    assert counts == [62] * 4
    for n, w in enumerate(W):
        sent(w.at[z, y, own_rows], csem.at[n])

        @pl.when(core == n % 2)
        def _(n=n, w=w):
            sent(w, wsem.at[n // 2, 0])
            sent(w.at[pl.ds(0, 7)], wsem.at[n // 2, 1])
            sent(w.at[0, pl.ds(0, 2)], wsem.at[n // 2, 2])
    sent(T.at[pl.ds(0, 576)], csem.at[4])
    sent(KV.at[pl.ds(0, 2)], csem.at[5])
    sent(ES, csem.at[6])
    sent(S2, csem.at[7])
    sent(S1, csem.at[8])
    sent(ST.at[:, pl.ds(0, 3)], csem.at[9])
    for cp in outs:
        cp.wait()


def body(
    tokens, query_weight, key_projection, value_projection, conv_in_weight, conv_gate_out,
    conv_gate_in, conv_taps, head_sink_logit, out_attn_weight, out_conv_weight, out_gain,
):
    half = HEAD // 2
    inverse = np.float32(THETA) ** (-np.arange(0, half, 2, dtype=np.float32) / np.float32(half))
    freq = jnp.asarray(np.tile(inverse.astype(np.float32), 4)[None, :])
    anywhere = pl.BlockSpec(memory_space=pl.ANY)
    specs = [anywhere] * 13
    specs[8] = pl.BlockSpec(memory_space=pltpu.SMEM)
    dma = pltpu.SemaphoreType.DMA
    return pl.pallas_call(
        kernel,
        out_shape=jax.ShapeDtypeStruct((ROWS, QUARTER), BF16),
        in_specs=specs,
        out_specs=anywhere,
        scratch_shapes=[
            pltpu.VMEM((ROWS, WIDTH), BF16),
            pltpu.VMEM((NZ, NY, 64, 512), BF16),
            pltpu.VMEM((NZ, NY, 64, 512), BF16),
            pltpu.VMEM((NZ, NY, 64, 256), BF16),
            pltpu.VMEM((NZ, NY, 64, 512), BF16),
            pltpu.VMEM((8, 128, 256), BF16),
            pltpu.VMEM((6, 256, 128), BF16),
            pltpu.VMEM((6, 128, 256), F32),
            pltpu.VMEM((6, 128, 256), F32),
            pltpu.VMEM((ROWS, QUARTER), BF16),
            pltpu.VMEM((2, 16, 256), BF16),
            pltpu.VMEM((2, 16, 256), BF16),
            pltpu.VMEM((ROWS, HEAD), F32),
            pltpu.VMEM((ROWS, HEAD), F32),
            pltpu.VMEM((3, 2, 128, QUARTER), BF16),
            pltpu.VMEM((3, 128, QUARTER), F32),
            pltpu.VMEM((3, 128, QUARTER), F32),
            pltpu.VMEM((3, 256, QUARTER), F32),
            pltpu.VMEM((3, 2, 2, 128, QUARTER), BF16),
            pltpu.VMEM((3, 2, 128, QUARTER), BF16),
            pltpu.VMEM((3, 2, 2, 128, QUARTER), BF16),
            pltpu.VMEM((3, 4, 2, 8, 128), F32),
            pltpu.VMEM((3, 256, QUARTER), BF16),
            pltpu.VMEM((3, 256), BF16),
            pltpu.VMEM((1, QUARTER), F32),
            pltpu.VMEM((1, HEAD), F32),
            dma((16,)),
            pltpu.SemaphoreType.REGULAR,
            dma((10,)),
            dma((2, 3)),
            dma((2, 32)),
            dma((2, 2)),
            dma((4,)),
            dma((14,)),
            dma((4,)),
            dma((6,)),
            dma((3,)),
            dma((3,)),
            dma((3,)),
        ],
        compiler_params=pltpu.CompilerParams(
            collective_id=0, has_side_effects=True, vmem_limit_bytes=56 * 1024 * 1024
        ),
    )(
        tokens, query_weight, key_projection, value_projection, conv_in_weight, conv_gate_out,
        conv_gate_in, conv_taps, head_sink_logit, out_attn_weight.T, out_conv_weight.T,
        out_gain.reshape(1, -1), freq,
    )


def solution(mesh):
    return jax.shard_map(
        body,
        mesh=mesh,
        in_specs=(
            P("sp", "tp"),
            P("sp", "tp"),
            P("sp", "tp"),
            P("sp", "tp"),
            P("sp", "tp"),
            P("sp", "tp"),
            P("sp", "tp"),
            P(None, "tp"),
            P("tp"),
            P("tp", "sp"),
            P("tp", "sp"),
            P("tp"),
        ),
        out_specs=P("sp", "tp"),
        check_vma=False,
    )
```

time: 84.6 us -> 77.6 us (0.917)
  Pallas kernels: 80.2 us -> 75.4 us
  local copies, waits for them, and re-layouts: 4.26 us -> 2.06 us
    pallas_call x1, Pallas kernels: 80.2 us -> 75.4 us  [body(): pl.pallas_call(kernel, out_shape=jax.ShapeDtypeStruct((ROWS, QUARTER), BF...]
    unnamed x5 -> x1, local copies, waits for them, and re-layouts: 4.26 us -> 2.06 us
where the time goes in v2:
time: 77.6 us; the launch traced here: 77.5 us
  Pallas kernels  75.4 us (97%)
  local copies, waits for them, and re-layouts  2.06 us (3%)
    pallas_call x1, Pallas kernels, body(): pl.pallas_call(kernel, out_shape=jax.ShapeDtypeStruct((ROWS, QUARTER), BF...  75.4 us
    unnamed x1, local copies, waits for them, and re-layouts  2.06 us

profile of v2, /device:TPU:2, one launch (start us, length us, event | category | flops | bytes accessed | tf_op | source)
XLA Modules:
  0.0 77.5 jit_solution(15581411894231305676)
XLA Ops:
  0.0 75.4 %shard_map.127 = bf16[768,512]{1,0:T(8,128)(2,1)} custom-call(bf16[768,512]{1,0:T(8,128)(2,1)} %tok.1, bf16[32,256]{1,0:T(8,128)(2,1)} %qw.1, bf16[32,128]{1,0:T(8,128)(2,1)} %kw.1, bf16[32,128]{1,0:T(8,128)(2,1)} %vw.1, bf16[32,256]{1,0:T(8,128)(2,1)} %cin.1, bf16[32,256]{1,0:T(8,128)(2,1)} %cgo.1, bf16[32,256]{1,0:T(8,128)(2,1)} %cgi.1, ...), custom_call_target="tpu_custom_call" | custom-call | tf_op jit(solution)/shard_map/pallas_call | solution.py:569
  75.4 2.1 %copy.15 = bf16[768,512]{1,0:T(8,128)(2,1)} copy(bf16[768,512]{1,0:T(8,128)(2,1)} %shard_map.127) | data formatting | bytes 1572864

commit v3 on v2

--- a/solution.py
+++ b/solution.py
@@ -24,6 +24,7 @@
 WIDTH = 2048
 QUARTER = 512
 ORDER = (0, 5, 1, 2, 3, 4)
+ICS = {0: 1, 1: 3, 3: 8}
 CHUNKS = ((0, 128, 0), (128, 128, 640), (256, 256, 128), (512, 256, 384))
 
 
@@ -32,10 +33,10 @@
 
 
 def kernel(
-    tok, qw, kw, vw, cin, cgo, cgi, taps_in, sink, owa, owc, gain_in, freq_in, out,
-    T, WA, WB, WC, WD, KV, Q, SEC, GA, MIX, ES, ER, COS, SIN, S2, PT, PB, PX, S1, R2, R1, ST, OUT,
-    taps_v, gain_v, freq_v,
-    lsem, met, csem, wsem, wrec, srec, irec, xrec, hrec, r2rec, r1rec, strec, osem,
+    tok, qw, kw, vw, cin, cgo, cgi, taps_in, sink_in, owa, owc, gain_in, freq_in, out,
+    T, WA, WB, WD, WOA, WOC, OWN, KV, Q, SEC, GA, MA, MC, ES, ER, COS, SIN, PX, ST,
+    taps_v, gain_v, freq_v, sink,
+    lsem, met, csem, wsem, wrec, srec, irec, xrec, hrec, mixrec, strec, osem, worec, wozrec, wozsem, woyrec, wosend, wosib,
 ):
     s = lax.axis_index("sp")
     x = lax.axis_index("tp")
@@ -69,15 +70,15 @@
         load(vw, WA.at[z, y, own_rows, pl.ds(384, 128)]),
         load(cin, WB.at[z, y, own_rows, pl.ds(0, 256)]),
         load(cgi, WB.at[z, y, own_rows, pl.ds(256, 256)]),
-        load(owa, WC.at[z, y, own_rows]),
-        load(cgo, WD.at[z, y, own_rows, pl.ds(0, 256)]),
-        load(owc, WD.at[z, y, own_rows, pl.ds(256, 256)]),
+        load(cgo, WD.at[z, y, own_rows]),
+        load(owa, OWN.at[0]),
+        load(owc, OWN.at[1]),
     ]
     l_t = [
         load(tok.at[pl.ds(src, n), :], T.at[pl.ds(dst, n), own_cols])
         for dst, n, src in CHUNKS
     ]
-    l_small = [load(taps_in, taps_v), load(gain_in, gain_v), load(freq_in, freq_v)]
+    l_small = [load(taps_in, taps_v), load(gain_in, gain_v), load(freq_in, freq_v), load(sink_in, sink)]
 
     barrier = pltpu.get_barrier_semaphore()
 
@@ -107,7 +108,7 @@
     def _():
         pl.semaphore_wait(met, 1)
 
-    counts = [0, 0, 0, 0]
+    counts = {0: 0, 1: 0, 3: 0}
 
     def copy(src, dst, rsem, peer, ssem):
         return pltpu.make_async_remote_copy(
@@ -136,9 +137,9 @@
         copy(ref, ref, rsem, xp, csem.at[0]).wait_recv()
 
     sib_rows = pl.ds(pl.multiple_of((1 - core) * 32, 32), 32)
-    W = (WA, WB, WC, WD)
-    for n, w in enumerate(W):
-        send(w.at[z, y, own_rows], w.at[z, y, own_rows], irec.at[n], sib, csem.at[n])
+    W = {0: WA, 1: WB, 3: WD}
+    for n, w in W.items():
+        send(w.at[z, y, own_rows], w.at[z, y, own_rows], irec.at[n], sib, csem.at[ICS[n]])
 
     def from_sib(n):
         arrived(W[n].at[z, y, sib_rows], irec.at[n])
@@ -287,6 +288,105 @@
         for dz in ring(k):
             got(n, dz, 2)
             to_sib(n, dz, 2)
+
+    WO = (WOA, WOC)
+    owner = z // 2
+    place = (z + NZ - 2 * x) % NZ
+    right = (place >= 1) & (place <= 4)
+    dist = jnp.where(right, place - 1, (NZ - place) % NZ)
+    u1 = jnp.where(right, 1, 0)
+    u2 = 1 - u1
+    onward = (at(z + jnp.where(right, 1, NZ - 1), y, core), x)
+    back = (at(z + jnp.where(right, NZ - 1, 1), y, core), x)
+
+    def wo_x():
+        for h in range(2):
+            here = (owner == x) & (core == h)
+
+            @pl.when(here)
+            def _(h=h):
+                WO[h][z % 2, y, x, own_rows, :] = OWN[h]
+
+            @pl.when(jnp.logical_not(here))
+            def _(h=h):
+                send(
+                    OWN.at[h], WO[h].at[z % 2, y, x, own_rows], worec.at[(x + NX - owner) % NX],
+                    (at(z, y, h), owner), csem.at[2 * h],
+                )
+
+    def wo_x_sent():
+        for h in range(2):
+            @pl.when(jnp.logical_not((owner == x) & (core == h)))
+            def _(h=h):
+                sent(OWN.at[h], csem.at[2 * h])
+
+    def wo_share(h, u):
+        unit = WO[h].at[u, y]
+        send(unit, unit, woyrec.at[0, u], yp, wosend.at[0])
+        send(unit, unit, woyrec.at[1, u], ym, wosend.at[0])
+        send(unit, unit, wosib.at[0], sib, wosend.at[2])
+
+    def wo_slot(h, k):
+        if k < 4:
+            @pl.when(dist == k)
+            def _():
+                unit = WO[h].at[u1, y]
+                if k == 0:
+                    arrived(WO[h].at[z % 2, y, x, sib_rows], worec.at[0])
+                    for d in (1, 2, 3):
+                        arrived(WO[h].at[z % 2, y, (x + d) % NX], worec.at[d])
+                    send(unit, unit, wozrec.at[1], back, wozsem.at[1])
+                else:
+                    arrived(unit, wozrec.at[0])
+                if k < 3:
+                    send(unit, unit, wozrec.at[0], onward, wozsem.at[0])
+                wo_share(h, u1)
+        if k > 0:
+            @pl.when(dist == k - 1)
+            def _():
+                unit = WO[h].at[u2, y]
+                arrived(unit, wozrec.at[1])
+                if k < 4:
+                    send(unit, unit, wozrec.at[1], onward, wozsem.at[2])
+                wo_share(h, u2)
+
+    def wo_y(h):
+        for u in range(2):
+            for d, o in ((3, 0), (1, 1)):
+                unit = WO[h].at[u, (y + d) % NY]
+                arrived(unit, woyrec.at[o, u])
+                if u == o:
+                    send(unit, unit, woyrec.at[2, u], yp if u == 0 else ym, wosend.at[1])
+                send(unit, unit, wosib.at[0], sib, wosend.at[2])
+
+    def wo_d(h):
+        for u in range(2):
+            unit = WO[h].at[u, (y + 2) % NY]
+            arrived(unit, woyrec.at[2, u])
+            send(unit, unit, wosib.at[0], sib, wosend.at[2])
+
+    def wo_end(h):
+        arrived(WO[1 - h], wosib.at[0])
+
+    def wo_sent():
+        unit = WOA.at[0, 0]
+        sent(WOA.at[0], wosend.at[0])
+        sent(WOA.at[0, pl.ds(0, 2)], wosend.at[1])
+        sent(WOA, wosend.at[2])
+
+        @pl.when(dist < 3)
+        def _():
+            sent(unit, wozsem.at[0])
+
+        @pl.when(dist < 4)
+        def _():
+            @pl.when(dist < 3)
+            def _():
+                sent(unit, wozsem.at[2])
+
+        @pl.when(dist == 0)
+        def _():
+            sent(unit, wozsem.at[1])
 
     for cp in l_small:
         cp.wait()
@@ -362,7 +462,7 @@
         before = jnp.where(row128 == 0, low, pltpu.roll(sec, 1, 0))
         later = jnp.where(row128 == 127, high, pltpu.roll(sec, 127, 0))
         mix = before * taps[0:1] + sec * taps[1:2] + later * taps[2:3]
-        MIX[b * 128 : (b + 1) * 128, 256:512] = (GA[b] * mix).astype(BF16)
+        MC[x, b * 128 : (b + 1) * 128, :] = (GA[b] * mix).astype(BF16)
 
     qi = lax.broadcasted_iota(jnp.int32, (256, 384), 0) % 128
     kj = lax.broadcasted_iota(jnp.int32, (256, 384), 1)
@@ -385,8 +485,8 @@
         probs = (w / total).astype(BF16)
         o = jnp.dot(probs, values, preferred_element_type=F32).astype(BF16)
         rows = slice(b * 128, b * 128 + 128)
-        MIX[rows, 0:HEAD] = o[:128]
-        MIX[rows, HEAD : 2 * HEAD] = o[128:]
+        MA[x, rows, 0:HEAD] = o[:128]
+        MA[x, rows, HEAD : 2 * HEAD] = o[128:]
 
     def halo_send():
         send(KV.at[1], KV.at[7], hrec.at[0], sm, csem.at[5])
@@ -406,44 +506,42 @@
         arrived(KV.at[7], hrec.at[0])
         arrived(ER.at[1], hrec.at[2])
 
+    M = (MA, MC)
+
+    def mix(h, d, r0, n):
+        return M[h].at[(x + d) % NX, pl.ds(r0, n)]
+
+    def mix_send(h, g):
+        blk = mix(h, 0, 256 * g, 256)
+        send(blk, blk, mixrec.at[2 * g + h, 0], xp, csem.at[7])
+        send(blk, blk, mixrec.at[2 * g + h, 1], xm, csem.at[7])
+
+    def mix_relay(h, g):
+        arrived(mix(h, 3, 256 * g, 256), mixrec.at[2 * g + h, 0])
+        blk = mix(h, 3, 256 * g, 128)
+        send(blk, blk, mixrec.at[2 * g + h, 2], xp, csem.at[7])
+        arrived(mix(h, 1, 256 * g, 256), mixrec.at[2 * g + h, 1])
+        blk = mix(h, 1, 256 * g + 128, 128)
+        send(blk, blk, mixrec.at[2 * g + h, 3], xm, csem.at[7])
+
     def partial(g, d):
         o = (x + d) % NX
-        a = MIX[256 * g : 256 * g + 256, 0:256]
-        c = MIX[256 * g : 256 * g + 256, 256:512]
-        wa = WC[pl.ds(2 * o, 2)].reshape(QUARTER, 256)
-        wb = WD[pl.ds(2 * o, 2), :, :, 256:512].reshape(QUARTER, 256)
-        return nt_dot(a, wa) + nt_dot(c, wb)
-
-    def spread_out(g):
-        p = partial(g, 2).astype(BF16)
-        S2[g, 0] = p[:128]
-        S2[g, 1] = p[128:]
-        send(S2.at[g, 0], R2.at[g, 0], r2rec.at[2 * g], xp, csem.at[7])
-        send(S2.at[g, 1], R2.at[g, 1], r2rec.at[2 * g + 1], xm, csem.at[7])
-        p = partial(g, 1)
-        PT[g] = p[:128]
-        S1[g, 0, 1] = p[128:].astype(BF16)
-        send(S1.at[g, 0, 1], R1.at[g, 0, 1], r1rec.at[g], xp, csem.at[8])
-        p = partial(g, 3)
-        PB[g] = p[128:]
-        S1[g, 1, 0] = p[:128].astype(BF16)
-        send(S1.at[g, 1, 0], R1.at[g, 1, 0], r1rec.at[g], xm, csem.at[8])
-        PX[g] = partial(g, 0)
-
-    def sum_relay(g):
-        arrived(R2.at[g, 0], r2rec.at[2 * g])
-        S1[g, 0, 0] = (PT[g] + R2[g, 0].astype(F32)).astype(BF16)
-        send(S1.at[g, 0, 0], R1.at[g, 0, 0], r1rec.at[g], xp, csem.at[8])
-        arrived(R2.at[g, 1], r2rec.at[2 * g + 1])
-        S1[g, 1, 1] = (PB[g] + R2[g, 1].astype(F32)).astype(BF16)
-        send(S1.at[g, 1, 1], R1.at[g, 1, 1], r1rec.at[g], xm, csem.at[8])
-
-    def local_stats(g):
-        arrived(R1.at[g], r1rec.at[g])
+        rows = slice(256 * g, 256 * g + 256)
+        return sum(
+            nt_dot(M[h][o, rows, :], WO[h][:, :, pl.ds(o, 1)].reshape(QUARTER, 256)) for h in range(2)
+        )
+
+    def final_near(g):
+        PX[g] = partial(g, 0) + partial(g, 1) + partial(g, 3)
+
+    def final_far(g):
+        for h in range(2):
+            arrived(mix(h, 2, 256 * g, 128), mixrec.at[2 * g + h, 2])
+            arrived(mix(h, 2, 256 * g + 128, 128), mixrec.at[2 * g + h, 3])
+        PX[g] += partial(g, 2)
         for half in range(2):
             rows = slice(128 * half, 128 * half + 128)
-            t = PX[g, rows, :] + R1[g, 0, half].astype(F32) + R1[g, 1, half].astype(F32)
-            PX[g, rows, :] = t
+            t = PX[g, rows, :]
             mean = jnp.sum(t, 1, keepdims=True) * (1.0 / QUARTER)
             m2 = jnp.sum(jnp.square(t - mean), 1, keepdims=True)
             lane = lax.broadcasted_iota(jnp.int32, (128, 128), 1)
@@ -466,79 +564,93 @@
             line = lax.broadcasted_iota(jnp.int32, (128, 128), 0)
             columns = jnp.transpose(jnp.where(line == 0, mean, scale))
             normed = (PX[g, rows, :] - columns[:, 0:1]) * columns[:, 1:2] * gain_v[0:1, :]
-            OUT[g, rows, :] = normed.astype(BF16)
-        cp = pltpu.make_async_copy(OUT.at[g], out.at[pl.ds(256 * g, 256), :], osem.at[g])
-        cp.start()
-        outs.append(cp)
+            out[256 * g + 128 * half : 256 * g + 128 * half + 128, :] = normed.astype(BF16)
 
     outs = []
     on_core(
         0,
-        (a_ysend, 0), (a_zsend, 0), (a_ysend, 2), (a_zsend, 2), (a_y, 0), (a_hop, 0, 1),
-        (x_relay, 0), (x_relay, 1), (x_send, 3),
-        (a_y, 2), (a_hop, 0, 2), (a_hop, 2, 1), (x_relay, 2),
-        (a_hop, 0, 3), (a_hop, 2, 2), (a_hop, 0, 4), (x_relay, 3),
+        (a_ysend, 0), (a_zsend, 0), (a_y, 0), (a_hop, 0, 1),
+        (x_relay, 0), (wo_x,), (x_relay, 1), (x_send, 3),
+        (a_hop, 0, 2), (x_relay, 2), (a_hop, 0, 3), (wo_slot, 0, 0), (a_hop, 0, 4), (x_relay, 3),
     )
     on_core(
         1,
         (b_start, 1), (b_zy, 1, 0), (b_start, 3),
         (b_z, 1, 1), (b_zy, 1, 1), (b_zy, 3, 0), (b_z, 3, 1), (b_zy, 3, 1),
         (b_z, 1, 2), (b_zy, 1, 2), (b_y, 1, 0), (b_z, 3, 2), (b_zy, 3, 2), (b_y, 3, 0), (b_y, 1, 1),
-        (x_relay, 0), (x_relay, 1), (x_send, 3),
+        (x_relay, 0), (wo_x,), (x_relay, 1), (x_send, 3),
         (b_z, 1, 3), (b_zy, 1, 3), (b_y, 3, 1), (b_z, 3, 3), (b_zy, 3, 3),
         (b_d, 1, 0), (b_d, 3, 0), (b_y, 1, 2), (b_d, 1, 1), (b_y, 3, 2),
         (b_z, 1, 4), (b_zy, 1, 4), (b_d, 3, 1), (b_z, 3, 4), (b_zy, 3, 4),
-        (x_relay, 2), (b_y, 1, 3), (b_y, 3, 3), (b_d, 1, 2), (b_d, 3, 2), (b_y, 1, 4), (b_y, 3, 4),
-        (x_relay, 3), (all_from_sib, 0),
+        (x_relay, 2), (b_y, 1, 3), (b_y, 3, 3), (wo_slot, 1, 0), (b_d, 1, 2), (b_d, 3, 2), (b_y, 1, 4), (b_y, 3, 4),
+        (x_relay, 3), (b_d, 1, 3), (b_d, 3, 3), (all_from_sib, 0),
     )
     x_rest(0)
     x_rest(1)
     project(0)
     halo_send()
-    on_core(0, (a_hop, 2, 3))
-    on_core(1, (b_d, 1, 3), (b_d, 3, 3))
+    on_core(0, (wo_slot, 0, 1))
+    on_core(1, (b_d, 1, 4), (b_d, 3, 4), (wo_slot, 1, 1))
     x_rest(2)
     project(1)
-    on_core(0, (a_hop, 2, 4))
-    on_core(1, (b_d, 1, 4), (b_d, 3, 4))
     attend(1)
     halo_left()
     attend(0)
+    mix_send(0, 0)
     on_core(0, (all_from_sib, 1), (all_from_sib, 3))
-    on_core(1, (all_from_sib, 2))
     project_conv(0)
     edge_send()
     project_conv(1)
     convolve(1)
     edge_left()
     convolve(0)
-    spread_out(0)
+    mix_send(1, 0)
+    on_core(0, (wo_slot, 0, 2))
+    on_core(1, (wo_slot, 1, 2))
     x_rest(3)
     project(2)
+    attend(2)
+    attend(3)
+    mix_send(0, 1)
+    mix_relay(0, 0)
     project_conv(2)
     convolve(2)
     convolve(3)
-    attend(2)
-    attend(3)
-    spread_out(1)
-    sum_relay(0)
-    convolve(4)
+    mix_send(1, 1)
+    on_core(0, (wo_slot, 0, 3))
+    on_core(1, (wo_slot, 1, 3))
+    mix_relay(1, 0)
     attend(4)
     halo_right()
+    attend(5)
+    mix_send(0, 2)
+    convolve(4)
     convolve(5)
-    attend(5)
-    spread_out(2)
-    sum_relay(1)
-    local_stats(0)
-    sum_relay(2)
-    local_stats(1)
-    local_stats(2)
+    mix_send(1, 2)
+    on_core(0, (wo_slot, 0, 4))
+    on_core(1, (wo_slot, 1, 4))
+    mix_relay(0, 1)
+    on_core(0, (wo_y, 0))
+    on_core(1, (wo_y, 1))
+    mix_relay(1, 1)
+    on_core(0, (wo_d, 0), (wo_end, 0))
+    on_core(1, (wo_d, 1), (wo_end, 1))
+    mix_relay(0, 2)
+    mix_relay(1, 2)
+    final_near(0)
+    final_far(0)
+    final_near(1)
+    final_far(1)
+    final_near(2)
+    final_far(2)
     finish(0)
     finish(1)
     finish(2)
-    assert counts == [62] * 4
-    for n, w in enumerate(W):
-        sent(w.at[z, y, own_rows], csem.at[n])
+    wo_x_sent()
+    wo_sent()
+    assert set(counts.values()) == {62}
+    for n, w in W.items():
+        sent(w.at[z, y, own_rows], csem.at[ICS[n]])
 
         @pl.when(core == n % 2)
         def _(n=n, w=w):
@@ -548,11 +660,8 @@
     sent(T.at[pl.ds(0, 576)], csem.at[4])
     sent(KV.at[pl.ds(0, 2)], csem.at[5])
     sent(ES, csem.at[6])
-    sent(S2, csem.at[7])
-    sent(S1, csem.at[8])
+    sent(T.at[pl.ds(0, 576)], csem.at[7])
     sent(ST.at[:, pl.ds(0, 3)], csem.at[9])
-    for cp in outs:
-        cp.wait()
 
 
 def body(
@@ -564,40 +673,36 @@
     freq = jnp.asarray(np.tile(inverse.astype(np.float32), 4)[None, :])
     anywhere = pl.BlockSpec(memory_space=pl.ANY)
     specs = [anywhere] * 13
-    specs[8] = pl.BlockSpec(memory_space=pltpu.SMEM)
     dma = pltpu.SemaphoreType.DMA
-    return pl.pallas_call(
+    call = pl.pallas_call(
         kernel,
         out_shape=jax.ShapeDtypeStruct((ROWS, QUARTER), BF16),
         in_specs=specs,
-        out_specs=anywhere,
+        out_specs=pl.BlockSpec(memory_space=pltpu.VMEM),
         scratch_shapes=[
             pltpu.VMEM((ROWS, WIDTH), BF16),
             pltpu.VMEM((NZ, NY, 64, 512), BF16),
             pltpu.VMEM((NZ, NY, 64, 512), BF16),
             pltpu.VMEM((NZ, NY, 64, 256), BF16),
-            pltpu.VMEM((NZ, NY, 64, 512), BF16),
+            pltpu.VMEM((2, NY, NX, 64, 256), BF16),
+            pltpu.VMEM((2, NY, NX, 64, 256), BF16),
+            pltpu.VMEM((2, 32, 256), BF16),
             pltpu.VMEM((8, 128, 256), BF16),
             pltpu.VMEM((6, 256, 128), BF16),
             pltpu.VMEM((6, 128, 256), F32),
             pltpu.VMEM((6, 128, 256), F32),
-            pltpu.VMEM((ROWS, QUARTER), BF16),
+            pltpu.VMEM((NX, ROWS, 256), BF16),
+            pltpu.VMEM((NX, ROWS, 256), BF16),
             pltpu.VMEM((2, 16, 256), BF16),
             pltpu.VMEM((2, 16, 256), BF16),
             pltpu.VMEM((ROWS, HEAD), F32),
             pltpu.VMEM((ROWS, HEAD), F32),
-            pltpu.VMEM((3, 2, 128, QUARTER), BF16),
-            pltpu.VMEM((3, 128, QUARTER), F32),
-            pltpu.VMEM((3, 128, QUARTER), F32),
             pltpu.VMEM((3, 256, QUARTER), F32),
-            pltpu.VMEM((3, 2, 2, 128, QUARTER), BF16),
-            pltpu.VMEM((3, 2, 128, QUARTER), BF16),
-            pltpu.VMEM((3, 2, 2, 128, QUARTER), BF16),
             pltpu.VMEM((3, 4, 2, 8, 128), F32),
-            pltpu.VMEM((3, 256, QUARTER), BF16),
             pltpu.VMEM((3, 256), BF16),
             pltpu.VMEM((1, QUARTER), F32),
             pltpu.VMEM((1, HEAD), F32),
+            pltpu.SMEM((2,), F32),
             dma((16,)),
             pltpu.SemaphoreType.REGULAR,
             dma((10,)),
@@ -607,19 +712,28 @@
             dma((4,)),
             dma((14,)),
             dma((4,)),
-            dma((6,)),
+            dma((6, 4)),
             dma((3,)),
+            dma((1,)),
+            dma((4,)),
+            dma((2,)),
             dma((3,)),
+            dma((3, 2)),
             dma((3,)),
+            dma((1,)),
         ],
         compiler_params=pltpu.CompilerParams(
-            collective_id=0, has_side_effects=True, vmem_limit_bytes=56 * 1024 * 1024
+            collective_id=0, has_side_effects=True, vmem_limit_bytes=40 * 1024 * 1024
         ),
-    )(
+    )
+    operands = [
         tokens, query_weight, key_projection, value_projection, conv_in_weight, conv_gate_out,
         conv_gate_in, conv_taps, head_sink_logit, out_attn_weight.T, out_conv_weight.T,
         out_gain.reshape(1, -1), freq,
-    )
+    ]
+    return call(*[
+        pltpu.with_memory_space_constraint(a, pltpu.HBM) for a in operands
+    ])
 
 
 def solution(mesh):

time: 77.6 us -> 72.5 us (0.934)
  Pallas kernels: 75.4 us -> 71.4 us
  local copies, waits for them, and re-layouts: 2.06 us -> 0.88 us
    pallas_call x1, Pallas kernels: 75.4 us -> 71.4 us  [body(): call(*[pltpu.with_memory_space_constraint(a, pltpu.HBM) for a in operands])]
    unnamed x1, local copies, waits for them, and re-layouts: 2.06 us -> 0.88 us
where the time goes in v3:
time: 72.5 us; the launch traced here: 72.3 us
  Pallas kernels  71.4 us (98%)
  local copies, waits for them, and re-layouts  0.88 us (1%)
    pallas_call x1, Pallas kernels, body(): call(*[pltpu.with_memory_space_constraint(a, pltpu.HBM) for a in operands])  71.4 us

profile of v3, /device:TPU:2, one launch (start us, length us, event | category | flops | bytes accessed | tf_op | source)
XLA Modules:
  0.0 72.3 jit_solution(16675872020037527266)
XLA Ops:
  0.0 71.4 %shard_map.127 = bf16[768,512]{1,0:T(8,128)(2,1)S(1)} custom-call(bf16[768,512]{1,0:T(8,128)(2,1)} %tok.1, bf16[32,256]{1,0:T(8,128)(2,1)} %qw.1, bf16[32,128]{1,0:T(8,128)(2,1)} %kw.1, bf16[32,128]{1,0:T(8,128)(2,1)} %vw.1, bf16[32,256]{1,0:T(8,128)(2,1)} %cin.1, bf16[32,256]{1,0:T(8,128)(2,1)} %cgo.1, bf16[32,256]{1,0:T(8,128)(2,1)} %cgi.1, ...), custom_call_target="tpu_custom_call" | custom-call | tf_op jit(solution)/shard_map/pallas_call | solution.py:734
  71.4 0.9 %copy.15 = bf16[768,512]{1,0:T(8,128)(2,1)} copy(bf16[768,512]{1,0:T(8,128)(2,1)S(1)} %shard_map.127) | data formatting | bytes 1572864

commit v4 on v3

--- a/solution.py
+++ b/solution.py
@@ -23,9 +23,8 @@
 ROWS = 768
 WIDTH = 2048
 QUARTER = 512
-ORDER = (0, 5, 1, 2, 3, 4)
+PLACED = (1, 2, 3, 4, 0, 5)
 ICS = {0: 1, 1: 3, 3: 8}
-CHUNKS = ((0, 128, 0), (128, 128, 640), (256, 256, 128), (512, 256, 384))
 
 
 def nt_dot(a, b):
@@ -75,8 +74,7 @@
         load(owc, OWN.at[1]),
     ]
     l_t = [
-        load(tok.at[pl.ds(src, n), :], T.at[pl.ds(dst, n), own_cols])
-        for dst, n, src in CHUNKS
+        load(tok.at[pl.ds(256 * m, 256), :], T.at[pl.ds(256 * m, 256), own_cols]) for m in range(3)
     ]
     l_small = [load(taps_in, taps_v), load(gain_in, gain_v), load(freq_in, freq_v), load(sink_in, sink)]
 
@@ -147,16 +145,33 @@
     def cols(d):
         return pl.ds(pl.multiple_of(((x + d) % NX) * QUARTER, QUARTER), QUARTER)
 
-    def x_send(i):
-        dst, n, _ = CHUNKS[i]
-        blk = T.at[pl.ds(dst, n), own_cols]
-        send(blk, blk, xrec.at[i], xp, csem.at[4])
-        send(blk, blk, xrec.at[4 + i], xm, csem.at[4])
-
-    for cp in l_t:
-        cp.wait()
-    for i in range(3):
-        x_send(i)
+    def t_block(b, d):
+        return T.at[pl.ds(128 * b, 128), cols(d)]
+
+    def x_send(m):
+        for b in (2 * m, 2 * m + 1):
+            send(t_block(b, 0), t_block(b, 0), xrec.at[0, b], xp, csem.at[4])
+        for b in (2 * m + 1, 2 * m):
+            send(t_block(b, 0), t_block(b, 0), xrec.at[1, b], xm, csem.at[4])
+
+    def x_relay(m):
+        b = 2 * m
+        arrived(t_block(b, 3), xrec.at[0, b])
+        send(t_block(b, 3), t_block(b, 3), xrec.at[2, b], xp, csem.at[4])
+        b = 2 * m + 1
+        arrived(t_block(b, 1), xrec.at[1, b])
+        send(t_block(b, 1), t_block(b, 1), xrec.at[2, b], xm, csem.at[4])
+
+    def x_rest(m):
+        arrived(t_block(2 * m, 1), xrec.at[1, 2 * m])
+        arrived(t_block(2 * m + 1, 3), xrec.at[0, 2 * m + 1])
+        for b in (2 * m, 2 * m + 1):
+            arrived(t_block(b, 2), xrec.at[2, b])
+
+    for m in range(2):
+        l_t[m].wait()
+        x_send(m)
+    l_t[2].wait()
 
     @pl.when(core == 1)
     def _():
@@ -166,40 +181,6 @@
     @pl.when(core == 0)
     def _():
         pl.semaphore_wait(met, 1)
-
-    RELAY = (
-        ((0, 0, 128, 1),),
-        ((1, 128, 128, -1),),
-        ((2, 256, 128, 1), (2, 384, 128, -1)),
-        ((3, 512, 128, 1), (3, 640, 128, -1)),
-    )
-
-    def t_chunk(i, d):
-        dst, n, _ = CHUNKS[i]
-        return T.at[pl.ds(dst, n), cols(d)]
-
-    def x_relay(i):
-        for _, r0, n, direction in RELAY[i]:
-            if direction == 1:
-                arrived(t_chunk(i, 3), xrec.at[i])
-                blk = T.at[pl.ds(r0, n), cols(3)]
-                send(blk, blk, xrec.at[8 + r0 // 128], xp, csem.at[4])
-            else:
-                arrived(t_chunk(i, 1), xrec.at[4 + i])
-                blk = T.at[pl.ds(r0, n), cols(1)]
-                send(blk, blk, xrec.at[8 + r0 // 128], xm, csem.at[4])
-
-    def x_rest(i):
-        if i == 0:
-            arrived(t_chunk(0, 1), xrec.at[4])
-            arrived(T.at[pl.ds(0, 128), cols(2)], xrec.at[8])
-        elif i == 1:
-            arrived(t_chunk(1, 3), xrec.at[1])
-            arrived(T.at[pl.ds(128, 128), cols(2)], xrec.at[9])
-        else:
-            r0 = CHUNKS[i][0]
-            arrived(T.at[pl.ds(r0, 128), cols(2)], xrec.at[8 + r0 // 128])
-            arrived(T.at[pl.ds(r0 + 128, 128), cols(2)], xrec.at[9 + r0 // 128])
 
     def rel(dz, dy):
         return (dz % NZ) * NY + dy % NY
@@ -240,8 +221,9 @@
             fwd(n, 0, dy, zm, 1, 0)
             to_sib(n, 0, dy)
 
-    def a_hop(n, k):
-        for i, dy in enumerate((0, 1, 3, 2)):
+    def a_hop(n, k, part=(0, 1, 2, 3)):
+        for i in part:
+            dy = (0, 1, 3, 2)[i]
             for dz in (-k, k) if k < 4 else (4,):
                 got(n, dz, dy)
                 if dz < 0 and (k < 3 or i % 2 == 0):
@@ -417,9 +399,8 @@
 
     def project(m):
         rows = slice(256 * m, 256 * m + 256)
-        blocks = ORDER[2 * m : 2 * m + 2]
-        cosine = jnp.concatenate([COS[b * 128 : b * 128 + 128, :] for b in blocks], 0)
-        sine = jnp.concatenate([SIN[b * 128 : b * 128 + 128, :] for b in blocks], 0)
+        blocks = (2 * m, 2 * m + 1)
+        cosine, sine = COS[rows, :], SIN[rows, :]
         q = jnp.dot(T[rows, :], weight(WA, 0), preferred_element_type=F32)
         for h in range(2):
             u = rotate(q[:, h * HEAD : (h + 1) * HEAD], cosine, sine)
@@ -434,20 +415,26 @@
 
     def project_conv(m):
         rows = slice(256 * m, 256 * m + 256)
-        blocks = ORDER[2 * m : 2 * m + 2]
+        blocks = (2 * m, 2 * m + 1)
         c_in = jnp.dot(T[rows, :], weight(WB, 0), preferred_element_type=F32)
         before = jnp.dot(T[rows, :], weight(WB, 256), preferred_element_type=F32)
         sec = (before * c_in).astype(BF16)
         for i, b in enumerate(blocks):
             SEC[b] = sec[i * 128 : (i + 1) * 128].astype(F32)
-            if m == 0:
-                ES[i] = sec[0:16] if i == 0 else sec[240:256]
+        if m == 0:
+            ES[0] = sec[0:16]
+        if m == 2:
+            ES[1] = sec[240:256]
         after = jnp.dot(T[rows, :], weight(WD, 0), preferred_element_type=F32)
         for i, b in enumerate(blocks):
             GA[b] = after[i * 128 : (i + 1) * 128]
 
     row128 = lax.broadcasted_iota(jnp.int32, (128, 1), 0)
     taps = taps_v[...].astype(F32)
+
+    def placed(b):
+        p = PLACED.index(b)
+        return slice(128 * p, 128 * p + 128)
 
     def convolve(b):
         sec = SEC[b]
@@ -462,7 +449,7 @@
         before = jnp.where(row128 == 0, low, pltpu.roll(sec, 1, 0))
         later = jnp.where(row128 == 127, high, pltpu.roll(sec, 127, 0))
         mix = before * taps[0:1] + sec * taps[1:2] + later * taps[2:3]
-        MC[x, b * 128 : (b + 1) * 128, :] = (GA[b] * mix).astype(BF16)
+        MC[x, placed(b), :] = (GA[b] * mix).astype(BF16)
 
     qi = lax.broadcasted_iota(jnp.int32, (256, 384), 0) % 128
     kj = lax.broadcasted_iota(jnp.int32, (256, 384), 1)
@@ -484,26 +471,28 @@
         total = jnp.sum(w, 1, keepdims=True) + jnp.exp(sink_col - top)
         probs = (w / total).astype(BF16)
         o = jnp.dot(probs, values, preferred_element_type=F32).astype(BF16)
-        rows = slice(b * 128, b * 128 + 128)
+        rows = placed(b)
         MA[x, rows, 0:HEAD] = o[:128]
         MA[x, rows, HEAD : 2 * HEAD] = o[128:]
 
-    def halo_send():
-        send(KV.at[1], KV.at[7], hrec.at[0], sm, csem.at[5])
-        send(KV.at[6], KV.at[0], hrec.at[1], sp, csem.at[5])
-
-    def edge_send():
-        send(ES.at[0], ER.at[1], hrec.at[2], sm, csem.at[6])
-        send(ES.at[1], ER.at[0], hrec.at[3], sp, csem.at[6])
-
-    def halo_left():
+    def halo_send(side):
+        if side == 0:
+            send(KV.at[1], KV.at[7], hrec.at[0], sm, csem.at[5])
+        else:
+            send(KV.at[6], KV.at[0], hrec.at[1], sp, csem.at[5])
+
+    def edge_send(side):
+        if side == 0:
+            send(ES.at[0], ER.at[1], hrec.at[2], sm, csem.at[6])
+        else:
+            send(ES.at[1], ER.at[0], hrec.at[3], sp, csem.at[6])
+
+    def halo_wait():
         arrived(KV.at[0], hrec.at[1])
-
-    def edge_left():
+        arrived(KV.at[7], hrec.at[0])
+
+    def edge_wait():
         arrived(ER.at[0], hrec.at[3])
-
-    def halo_right():
-        arrived(KV.at[7], hrec.at[0])
         arrived(ER.at[1], hrec.at[2])
 
     M = (MA, MC)
@@ -564,67 +553,67 @@
             line = lax.broadcasted_iota(jnp.int32, (128, 128), 0)
             columns = jnp.transpose(jnp.where(line == 0, mean, scale))
             normed = (PX[g, rows, :] - columns[:, 0:1]) * columns[:, 1:2] * gain_v[0:1, :]
-            out[256 * g + 128 * half : 256 * g + 128 * half + 128, :] = normed.astype(BF16)
+            out[PLACED[2 * g + half] * 128 : PLACED[2 * g + half] * 128 + 128, :] = normed.astype(BF16)
 
     outs = []
     on_core(
         0,
         (a_ysend, 0), (a_zsend, 0), (a_y, 0), (a_hop, 0, 1),
-        (x_relay, 0), (wo_x,), (x_relay, 1), (x_send, 3),
-        (a_hop, 0, 2), (x_relay, 2), (a_hop, 0, 3), (wo_slot, 0, 0), (a_hop, 0, 4), (x_relay, 3),
+        (x_relay, 0), (wo_x,), (x_relay, 1), (x_send, 2),
+        (a_hop, 0, 2), (a_hop, 0, 3), (wo_slot, 0, 0), (a_hop, 0, 4),
     )
     on_core(
         1,
         (b_start, 1), (b_zy, 1, 0), (b_start, 3),
         (b_z, 1, 1), (b_zy, 1, 1), (b_zy, 3, 0), (b_z, 3, 1), (b_zy, 3, 1),
         (b_z, 1, 2), (b_zy, 1, 2), (b_y, 1, 0), (b_z, 3, 2), (b_zy, 3, 2), (b_y, 3, 0), (b_y, 1, 1),
-        (x_relay, 0), (wo_x,), (x_relay, 1), (x_send, 3),
+        (x_relay, 0), (wo_x,), (x_relay, 1), (x_send, 2),
         (b_z, 1, 3), (b_zy, 1, 3), (b_y, 3, 1), (b_z, 3, 3), (b_zy, 3, 3),
         (b_d, 1, 0), (b_d, 3, 0), (b_y, 1, 2), (b_d, 1, 1), (b_y, 3, 2),
         (b_z, 1, 4), (b_zy, 1, 4), (b_d, 3, 1), (b_z, 3, 4), (b_zy, 3, 4),
-        (x_relay, 2), (b_y, 1, 3), (b_y, 3, 3), (wo_slot, 1, 0), (b_d, 1, 2), (b_d, 3, 2), (b_y, 1, 4), (b_y, 3, 4),
-        (x_relay, 3), (b_d, 1, 3), (b_d, 3, 3), (all_from_sib, 0),
+        (b_y, 1, 3), (b_y, 3, 3), (wo_slot, 1, 0), (b_d, 1, 2), (b_d, 3, 2), (b_y, 1, 4), (b_y, 3, 4),
+        (b_d, 1, 3), (b_d, 3, 3), (all_from_sib, 0),
     )
     x_rest(0)
+    project(0)
+    halo_send(0)
+    on_core(0, (x_relay, 2), (wo_slot, 0, 1))
+    on_core(1, (x_relay, 2), (b_d, 1, 4), (b_d, 3, 4), (wo_slot, 1, 1))
     x_rest(1)
-    project(0)
-    halo_send()
-    on_core(0, (wo_slot, 0, 1))
-    on_core(1, (b_d, 1, 4), (b_d, 3, 4), (wo_slot, 1, 1))
-    x_rest(2)
     project(1)
     attend(1)
-    halo_left()
-    attend(0)
+    attend(2)
     mix_send(0, 0)
     on_core(0, (all_from_sib, 1), (all_from_sib, 3))
     project_conv(0)
-    edge_send()
+    edge_send(0)
     project_conv(1)
     convolve(1)
-    edge_left()
-    convolve(0)
+    convolve(2)
     mix_send(1, 0)
     on_core(0, (wo_slot, 0, 2))
     on_core(1, (wo_slot, 1, 2))
-    x_rest(3)
+    x_rest(2)
     project(2)
-    attend(2)
+    halo_send(1)
     attend(3)
+    attend(4)
     mix_send(0, 1)
     mix_relay(0, 0)
     project_conv(2)
-    convolve(2)
+    edge_send(1)
     convolve(3)
+    convolve(4)
     mix_send(1, 1)
     on_core(0, (wo_slot, 0, 3))
     on_core(1, (wo_slot, 1, 3))
     mix_relay(1, 0)
-    attend(4)
-    halo_right()
+    halo_wait()
+    attend(0)
     attend(5)
     mix_send(0, 2)
-    convolve(4)
+    edge_wait()
+    convolve(0)
     convolve(5)
     mix_send(1, 2)
     on_core(0, (wo_slot, 0, 4))
@@ -710,7 +699,7 @@
             dma((2, 32)),
             dma((2, 2)),
             dma((4,)),
-            dma((14,)),
+            dma((3, 6)),
             dma((4,)),
             dma((6, 4)),
             dma((3,)),

time: 72.5 us -> 68.6 us (0.946); the launches traced: 72.3 us -> 67.2 us
  Pallas kernels: 71.4 us -> 66.4 us
    pallas_call x1, Pallas kernels: 71.4 us -> 66.4 us  [body(): call(*[pltpu.with_memory_space_constraint(a, pltpu.HBM) for a in operands])]
where the time goes in v4:
time: 68.6 us; the launch traced here: 67.2 us
  Pallas kernels  66.4 us (97%)
  local copies, waits for them, and re-layouts  0.88 us (1%)
    pallas_call x1, Pallas kernels, body(): call(*[pltpu.with_memory_space_constraint(a, pltpu.HBM) for a in operands])  66.4 us

profile of v4, /device:TPU:2, one launch (start us, length us, event | category | flops | bytes accessed | tf_op | source)
XLA Modules:
  0.0 67.2 jit_solution(16919548163462362647)
XLA Ops:
  0.0 66.4 %shard_map.127 = bf16[768,512]{1,0:T(8,128)(2,1)S(1)} custom-call(bf16[768,512]{1,0:T(8,128)(2,1)} %tok.1, bf16[32,256]{1,0:T(8,128)(2,1)} %qw.1, bf16[32,128]{1,0:T(8,128)(2,1)} %kw.1, bf16[32,128]{1,0:T(8,128)(2,1)} %vw.1, bf16[32,256]{1,0:T(8,128)(2,1)} %cin.1, bf16[32,256]{1,0:T(8,128)(2,1)} %cgo.1, bf16[32,256]{1,0:T(8,128)(2,1)} %cgi.1, ...), custom_call_target="tpu_custom_call" | custom-call | tf_op jit(solution)/shard_map/pallas_call | solution.py:723
  66.4 0.9 %copy.15 = bf16[768,512]{1,0:T(8,128)(2,1)} copy(bf16[768,512]{1,0:T(8,128)(2,1)S(1)} %shard_map.127) | data formatting | bytes 1572864

commit v5 on v4

--- a/solution.py
+++ b/solution.py
@@ -149,24 +149,22 @@
         return T.at[pl.ds(128 * b, 128), cols(d)]
 
     def x_send(m):
-        for b in (2 * m, 2 * m + 1):
-            send(t_block(b, 0), t_block(b, 0), xrec.at[0, b], xp, csem.at[4])
-        for b in (2 * m + 1, 2 * m):
-            send(t_block(b, 0), t_block(b, 0), xrec.at[1, b], xm, csem.at[4])
+        a, b = t_block(2 * m, 0), t_block(2 * m + 1, 0)
+        send(a, a, xrec.at[0, m], xp, csem.at[4])
+        send(b, b, xrec.at[2, m], xp, csem.at[4])
+        send(b, b, xrec.at[1, m], xm, csem.at[4])
+        send(a, a, xrec.at[2, m], xm, csem.at[4])
 
     def x_relay(m):
         b = 2 * m
-        arrived(t_block(b, 3), xrec.at[0, b])
-        send(t_block(b, 3), t_block(b, 3), xrec.at[2, b], xp, csem.at[4])
+        arrived(t_block(b, 3), xrec.at[0, m])
+        send(t_block(b, 3), t_block(b, 3), xrec.at[2, m], xp, csem.at[4])
         b = 2 * m + 1
-        arrived(t_block(b, 1), xrec.at[1, b])
-        send(t_block(b, 1), t_block(b, 1), xrec.at[2, b], xm, csem.at[4])
+        arrived(t_block(b, 1), xrec.at[1, m])
+        send(t_block(b, 1), t_block(b, 1), xrec.at[2, m], xm, csem.at[4])
 
     def x_rest(m):
-        arrived(t_block(2 * m, 1), xrec.at[1, 2 * m])
-        arrived(t_block(2 * m + 1, 3), xrec.at[0, 2 * m + 1])
-        for b in (2 * m, 2 * m + 1):
-            arrived(t_block(b, 2), xrec.at[2, b])
+        arrived(T.at[pl.ds(0, 128)], xrec.at[2, m])
 
     for m in range(2):
         l_t[m].wait()
@@ -511,7 +509,7 @@
         send(blk, blk, mixrec.at[2 * g + h, 2], xp, csem.at[7])
         arrived(mix(h, 1, 256 * g, 256), mixrec.at[2 * g + h, 1])
         blk = mix(h, 1, 256 * g + 128, 128)
-        send(blk, blk, mixrec.at[2 * g + h, 3], xm, csem.at[7])
+        send(blk, blk, mixrec.at[2 * g + h, 2], xm, csem.at[7])
 
     def partial(g, d):
         o = (x + d) % NX
@@ -525,8 +523,7 @@
 
     def final_far(g):
         for h in range(2):
-            arrived(mix(h, 2, 256 * g, 128), mixrec.at[2 * g + h, 2])
-            arrived(mix(h, 2, 256 * g + 128, 128), mixrec.at[2 * g + h, 3])
+            arrived(mix(h, 2, 256 * g, 256), mixrec.at[2 * g + h, 2])
         PX[g] += partial(g, 2)
         for half in range(2):
             rows = slice(128 * half, 128 * half + 128)
@@ -626,6 +623,20 @@
     on_core(1, (wo_d, 1), (wo_end, 1))
     mix_relay(0, 2)
     mix_relay(1, 2)
+    wo_x_sent()
+    wo_sent()
+    assert set(counts.values()) == {62}
+    for n, w in W.items():
+        sent(w.at[z, y, own_rows], csem.at[ICS[n]])
+
+        @pl.when(core == n % 2)
+        def _(n=n, w=w):
+            sent(w, wsem.at[n // 2, 0])
+            sent(w.at[pl.ds(0, 7)], wsem.at[n // 2, 1])
+            sent(w.at[0, pl.ds(0, 2)], wsem.at[n // 2, 2])
+    sent(T.at[pl.ds(0, 576)], csem.at[4])
+    sent(KV.at[pl.ds(0, 2)], csem.at[5])
+    sent(ES, csem.at[6])
     final_near(0)
     final_far(0)
     final_near(1)
@@ -635,20 +646,6 @@
     finish(0)
     finish(1)
     finish(2)
-    wo_x_sent()
-    wo_sent()
-    assert set(counts.values()) == {62}
-    for n, w in W.items():
-        sent(w.at[z, y, own_rows], csem.at[ICS[n]])
-
-        @pl.when(core == n % 2)
-        def _(n=n, w=w):
-            sent(w, wsem.at[n // 2, 0])
-            sent(w.at[pl.ds(0, 7)], wsem.at[n // 2, 1])
-            sent(w.at[0, pl.ds(0, 2)], wsem.at[n // 2, 2])
-    sent(T.at[pl.ds(0, 576)], csem.at[4])
-    sent(KV.at[pl.ds(0, 2)], csem.at[5])
-    sent(ES, csem.at[6])
     sent(T.at[pl.ds(0, 576)], csem.at[7])
     sent(ST.at[:, pl.ds(0, 3)], csem.at[9])
 
@@ -699,9 +696,9 @@
             dma((2, 32)),
             dma((2, 2)),
             dma((4,)),
-            dma((3, 6)),
+            dma((3, 3)),
             dma((4,)),
-            dma((6, 4)),
+            dma((6, 3)),
             dma((3,)),
             dma((1,)),
             dma((4,)),

time: 68.6 us -> 68.4 us (level)
  no operation moved by 1% of the time
where the time goes in v5:
time: 68.4 us; the launch traced here: 67.1 us
  Pallas kernels  66.2 us (97%)
  local copies, waits for them, and re-layouts  0.88 us (1%)
    pallas_call x1, Pallas kernels, body(): call(*[pltpu.with_memory_space_constraint(a, pltpu.HBM) for a in operands])  66.2 us

profile of v5, /device:TPU:2, one launch (start us, length us, event | category | flops | bytes accessed | tf_op | source)
XLA Modules:
  0.0 67.1 jit_solution(234704121355469639)
XLA Ops:
  0.0 66.2 %shard_map.127 = bf16[768,512]{1,0:T(8,128)(2,1)S(1)} custom-call(bf16[768,512]{1,0:T(8,128)(2,1)} %tok.1, bf16[32,256]{1,0:T(8,128)(2,1)} %qw.1, bf16[32,128]{1,0:T(8,128)(2,1)} %kw.1, bf16[32,128]{1,0:T(8,128)(2,1)} %vw.1, bf16[32,256]{1,0:T(8,128)(2,1)} %cin.1, bf16[32,256]{1,0:T(8,128)(2,1)} %cgo.1, bf16[32,256]{1,0:T(8,128)(2,1)} %cgi.1, ...), custom_call_target="tpu_custom_call" | custom-call | tf_op jit(solution)/shard_map/pallas_call | solution.py:720
  66.2 0.9 %copy.15 = bf16[768,512]{1,0:T(8,128)(2,1)} copy(bf16[768,512]{1,0:T(8,128)(2,1)S(1)} %shard_map.127) | data formatting | bytes 1572864

commit v6 on v5

--- a/solution.py
+++ b/solution.py
@@ -568,8 +568,8 @@
         (b_z, 1, 3), (b_zy, 1, 3), (b_y, 3, 1), (b_z, 3, 3), (b_zy, 3, 3),
         (b_d, 1, 0), (b_d, 3, 0), (b_y, 1, 2), (b_d, 1, 1), (b_y, 3, 2),
         (b_z, 1, 4), (b_zy, 1, 4), (b_d, 3, 1), (b_z, 3, 4), (b_zy, 3, 4),
-        (b_y, 1, 3), (b_y, 3, 3), (wo_slot, 1, 0), (b_d, 1, 2), (b_d, 3, 2), (b_y, 1, 4), (b_y, 3, 4),
-        (b_d, 1, 3), (b_d, 3, 3), (all_from_sib, 0),
+        (b_y, 1, 3), (b_y, 3, 3), (b_d, 1, 2), (b_d, 3, 2), (b_y, 1, 4), (b_y, 3, 4),
+        (b_d, 1, 3), (b_d, 3, 3), (wo_slot, 1, 0), (all_from_sib, 0),
     )
     x_rest(0)
     project(0)

time: 68.4 us -> 68.5 us (level)
  the two profiles are of different devices: /device:TPU:2 before, /device:TPU:8 now
where the time goes in v6:
time: 68.5 us; the launch traced here: 68.3 us
  Pallas kernels  67.4 us (98%)
  local copies, waits for them, and re-layouts  0.88 us (1%)
    pallas_call x1, Pallas kernels, body(): call(*[pltpu.with_memory_space_constraint(a, pltpu.HBM) for a in operands])  67.4 us

profile of v6, /device:TPU:8, one launch (start us, length us, event | category | flops | bytes accessed | tf_op | source)
XLA Modules:
  0.0 68.3 jit_solution(2301751141184604167)
XLA Ops:
  0.0 67.4 %shard_map.127 = bf16[768,512]{1,0:T(8,128)(2,1)S(1)} custom-call(bf16[768,512]{1,0:T(8,128)(2,1)} %tok.1, bf16[32,256]{1,0:T(8,128)(2,1)} %qw.1, bf16[32,128]{1,0:T(8,128)(2,1)} %kw.1, bf16[32,128]{1,0:T(8,128)(2,1)} %vw.1, bf16[32,256]{1,0:T(8,128)(2,1)} %cin.1, bf16[32,256]{1,0:T(8,128)(2,1)} %cgo.1, bf16[32,256]{1,0:T(8,128)(2,1)} %cgi.1, ...), custom_call_target="tpu_custom_call" | custom-call | tf_op jit(solution)/shard_map/pallas_call | solution.py:720
  67.4 0.9 %copy.15 = bf16[768,512]{1,0:T(8,128)(2,1)} copy(bf16[768,512]{1,0:T(8,128)(2,1)S(1)} %shard_map.127) | data formatting | bytes 1572864
